TPU v7x, 256 devices: a whole 4x4x8 slice. The times are simulated.
256 devices in a mesh: tp: 16 (over y, x), dp: 16 (over z, core).
Axes of the slice: x: 4, y: 4, z: 8, core: 2. Of those that a mesh axis runs over, the one named last changes fastest.
Arguments:
- tokens: bfloat16 [256, 4096], P(None, 'dp'), may hold values from -15 to 15, as said below
- norm_gain: float32 [2, 4096], P(None, 'dp'), may hold values from 0.1 to 1.9
- w_query: bfloat16 [2, 4096, 2048], P(None, 'dp', 'tp'), may hold values from -0.09375 to 0.09375
- w_forget: bfloat16 [2, 4096, 2048], P(None, 'dp', 'tp'), may hold values from -0.09375 to 0.09375
- w_value: bfloat16 [2, 4096, 2048], P(None, 'dp', 'tp'), may hold values from -0.09375 to 0.09375
- w_gate: bfloat16 [2, 4096, 2048], P(None, 'dp', 'tp'), may hold values from -0.09375 to 0.09375
- floor_rate: float32 [2, 2048], P(None, 'tp'), may hold values from 0 to 0.9
- head_gain: float32 [2, 128], replicated, may hold values from 0.1 to 1.9
- w_output: bfloat16 [2, 2048, 4096], P(None, 'tp', 'dp'), may hold values from -0.3 to 0.3
- state: float32 [2, 256, 16, 128, 128], P(None, 'dp', 'tp'), may hold values from -4 to 4
Outputs:
- mixed: bfloat16 [256, 4096], P(None, 'dp')
- new_state: float32 [2, 256, 16, 128, 128], P(None, 'dp', 'tp')
Inputs may be any that keep to these rules, and one draw needn't show every extreme that they name: `tokens`: activations whose feature blocks have different scales.
All inputs are finite; a program needn't handle non-finite values.
Results may differ from a plain program's by a relative error of at most 0.035.
Values may be sent and summed in bfloat16 or wider, within the bound.
No kernel may reach another device: no remote copies, remote signals or barrier semaphores. Data moves between devices by JAX's collectives and lax.ppermute only.
A program may use at most 64 MiB of HBM per device.

v0:
```python
import functools

import jax
import jax.numpy as jnp
from jax import lax
from jax.experimental import pallas as pl
from jax.experimental.pallas import tpu as pltpu
from jax.sharding import Mesh
from jax.sharding import PartitionSpec as P


D = 4096
EPS = 1e-06
BF16 = jnp.bfloat16
F32 = jnp.float32
LANES = 128


LANES_COST = 10**10


def call(kernel, outs, *args, flops=0):
    vmem = pl.BlockSpec(memory_space=pltpu.VMEM)
    size = sum(a.size * a.dtype.itemsize for a in args)
    return pl.pallas_call(
        kernel,
        out_shape=outs,
        in_specs=[vmem] * len(args),
        out_specs=[vmem] * len(outs),
        cost_estimate=pl.CostEstimate(flops=flops, bytes_accessed=size, transcendentals=0),
        compiler_params=pltpu.CompilerParams(vmem_limit_bytes=12 * 2**20),
    )(*args)


def rounded(x):
    return x.astype(BF16).astype(F32)


def project(x, gain, weights):
    x = x.astype(F32)
    normed = (x * gain).astype(BF16)
    products = [jnp.dot(normed, w, preferred_element_type=F32) for w in weights]
    return products, jnp.sum(x * x, axis=1, keepdims=True)


def in_three(squares, lanes):
    high = rounded(squares)
    middle = rounded(squares - high)
    low = squares - high - middle
    return high * lanes[0:1] + middle * lanes[1:2] + low * lanes[2:3]


def store(totals, squares, lanes, payload_ref):
    n_z, own_rows, _ = payload_ref.shape
    for p, part in enumerate([*totals, in_three(squares, lanes)]):
        payload_ref[:, :, p * LANES : (p + 1) * LANES] = (
            part.astype(BF16).reshape(n_z, own_rows, LANES)
        )


def start_kernel(lanes, tok, gain, floor_rate, head_gain, *refs):
    w, (keep_ref, send_ref, bundle_ref, rates_ref) = refs[0:4], refs[4:]
    core = lax.axis_index("c")
    n_z, _, own_rows, feats = tok.shape
    rows = n_z * own_rows
    weights = [v[0] for v in w]
    gain_0 = gain[0:1, :]
    x = tok[:, 1 - core].reshape(rows, feats)
    bundle_ref[0:rows, 4 * LANES :] = x
    store(*project(x, gain_0, weights), lanes, send_ref)
    x = tok[:, core].reshape(rows, feats)
    totals, squares = project(x, gain_0, weights)
    for p in range(4):
        keep_ref[:, p * LANES : (p + 1) * LANES] = totals[p]
        bundle_ref[:, p * LANES : (p + 1) * LANES] = w[p][1]
    keep_ref[:, 4 * LANES :] = in_three(squares, lanes)
    rates_ref[0:2] = floor_rate[...]
    rates_ref[2:4] = head_gain[...]
    gain_1 = gain[1:2, :]
    high = rounded(gain_1)
    middle = rounded(gain_1 - high)
    for n, term in enumerate((high, middle, gain_1 - high - middle)):
        bundle_ref[rows + 16 * n : rows + 16 * n + 16, 4 * LANES :] = jnp.broadcast_to(
            term, (16, feats)
        ).astype(BF16)


def lanes_kernel(out_ref):
    row = lax.broadcasted_iota(jnp.int32, out_ref.shape, 0)
    lane = lax.broadcasted_iota(jnp.int32, out_ref.shape, 1)
    out_ref[...] = jnp.where(row == lane, 1.0, 0.0)


def pair_kernel(lanes, keep, received, payload_ref):
    n_z, own_rows, width = received.shape
    total = keep[...] + received[...].reshape(n_z * own_rows, width).astype(F32)
    extra = total[:, 4 * LANES :]
    squares = extra[:, 0:1] + extra[:, 1:2] + extra[:, 2:3]
    parts = [total[:, p * LANES : (p + 1) * LANES] for p in range(4)]
    store(parts, squares, lanes, payload_ref)


def add_up(parts, halves):
    terms = [p[...].astype(F32) for p in parts]
    update = (terms[0] + terms[1]) + (terms[2] + terms[3])
    feats = halves[0].shape[1]
    return [
        (half.astype(F32) + update[:, n * feats : (n + 1) * feats]).astype(BF16)
        for n, half in enumerate(halves)
    ]


def middle_kernel(p0, p1, p2, p3, lanes, tok, gain, *refs):
    w, (bundle, payload_ref, x_ref) = refs[0:4], refs[4:]
    core = lax.axis_index("c")
    n_z, _, own_rows, feats = tok.shape
    rows = n_z * own_rows
    mine = tok[:, core].reshape(rows, feats)
    halves = add_up((p0, p1, p2, p3), [mine, bundle[0:rows, 4 * LANES :]])
    other_gain = sum(
        bundle[rows + 16 * n : rows + 16 * n + 16, 4 * LANES :][0:1].astype(F32) for n in range(3)
    )
    totals, squares = project(halves[0], gain[1:2, :], [v[1] for v in w])
    other_w = [bundle[:, p * LANES : (p + 1) * LANES] for p in range(4)]
    others, other_squares = project(halves[1], other_gain, other_w)
    store([t + o for t, o in zip(totals, others)], squares + other_squares, lanes, payload_ref)
    x_ref[0] = halves[0]
    x_ref[1] = halves[1]


def last_kernel(*refs):
    parts, (x_in, keep_ref, send_ref) = refs[0:4], refs[4:]
    halves = add_up(parts, [x_in[0], x_in[1]])
    keep_ref[...] = halves[0]
    send_ref[...] = halves[1]


def join_kernel(keep, received, out_ref):
    core = lax.axis_index("c")
    n_z, _, own_rows, feats = out_ref.shape
    out_ref[:, core] = keep[...].reshape(n_z, own_rows, feats)
    out_ref[:, 1 - core] = received[...].reshape(n_z, own_rows, feats)


def sigmoid(x):
    return 1.0 / (1.0 + jnp.exp(-x))


def mix_kernel(layer, arrived, rates, state, gated_ref, terms_ref):
    summed = arrived[0].astype(F32)
    for n in range(1, arrived.shape[0]):
        summed = summed + arrived[n].astype(F32)
    own_rows = summed.shape[0]
    extra = summed[:, 4 * LANES :]
    square = extra[:, 0:1] + extra[:, 1:2] + extra[:, 2:3]
    row_scale = lax.rsqrt(square / D + EPS)
    query_pre, forget_pre, value, gate_pre = [
        row_scale * summed[:, p * LANES : (p + 1) * LANES] for p in range(4)
    ]
    floor = rates[layer : layer + 1, :]
    query = query_pre * sigmoid(query_pre) * LANES ** (-0.5)
    forget = floor + (1.0 - floor) * sigmoid(forget_pre)
    key_in = (1.0 - floor) * sigmoid(-forget_pre)
    terms_ref[0] = forget
    terms_ref[1] = key_in
    terms_ref[2] = value
    columns = (query * forget).T
    fresh = jnp.sum(query * key_in, axis=1, keepdims=True) * value
    kept = [
        jnp.sum(state[layer, i, 0] * columns[:, i : i + 1], axis=0, keepdims=True)
        for i in range(own_rows)
    ]
    read = jnp.concatenate(kept, axis=0) + fresh
    read = read * lax.rsqrt(jnp.mean(read * read, axis=1, keepdims=True) + EPS)
    gate = gate_pre * sigmoid(gate_pre)
    gated = (read * rates[layer + 2 : layer + 3, :] * gate).astype(BF16)
    for n in range(gated_ref.shape[0]):
        gated_ref[n] = gated


def update_kernel(terms_a, terms_b, state, out_ref):
    def write(terms):
        forget = terms[0].T
        key_in = terms[1].T
        for i in range(state.shape[1]):
            value = terms[2, i : i + 1, :]
            out_ref[0, i, 0] = state[0, i, 0] * forget[:, i : i + 1] + key_in[:, i : i + 1] * value

    @pl.when(pl.program_id(0) == 0)
    def _():
        write(terms_a)

    @pl.when(pl.program_id(0) == 1)
    def _():
        write(terms_b)


def new_states(terms_a, terms_b, state):
    layers, seqs, heads, dk, dv = state.shape
    step = 8
    terms_spec = pl.BlockSpec((3, step, dk), lambda l, i: (0, i, 0))
    state_spec = pl.BlockSpec((1, step, heads, dk, dv), lambda l, i: (l, i, 0, 0, 0))
    return pl.pallas_call(
        update_kernel,
        out_shape=jax.ShapeDtypeStruct(state.shape, F32),
        grid=(layers, seqs // step),
        in_specs=[terms_spec, terms_spec, state_spec],
        out_specs=state_spec,
        cost_estimate=pl.CostEstimate(flops=10**7, bytes_accessed=2 * state.size * 4, transcendentals=0),
        compiler_params=pltpu.CompilerParams(vmem_limit_bytes=12 * 2**20),
        name="new_states",
    )(terms_a, terms_b, state)


def output_kernel(layer, heads, w_a, w_b, out_ref):
    my_x = lax.axis_index("x")
    n_x = heads.shape[0]
    rows = heads.shape[1] * heads.shape[2]
    for half, w in enumerate((w_a, w_b)):
        total = None
        for i in range(n_x):
            block = w[lax.rem(my_x - i + n_x, n_x), layer]
            product = jnp.dot(
                heads[i].reshape(rows, LANES), block, preferred_element_type=F32
            )
            total = product if total is None else total + product
        total = total.astype(BF16)
        feats = total.shape[1]
        out_ref[:, half * feats : (half + 1) * feats] = total


def spread(copies, axes):
    return lax.all_to_all(copies, axes, split_axis=0, concat_axis=0, tiled=True)


def per_device(
    tokens, norm_gain, w_query, w_forget, w_value, w_gate, floor_rate, head_gain, w_output, state
):
    n_z, n_x, n_y = lax.axis_size("z"), lax.axis_size("x"), lax.axis_size("y")
    batch, feats = tokens.shape
    own_rows = batch // (2 * n_z)
    rows = n_z * own_rows

    def swap(v):
        return lax.ppermute(v, "c", [(0, 1), (1, 0)])

    weights = (w_query, w_forget, w_value, w_gate)
    tok = tokens.reshape(n_z, 2, own_rows, feats)
    payload_shape = jax.ShapeDtypeStruct((n_z, own_rows, 5 * LANES), BF16)
    x_shape = jax.ShapeDtypeStruct((2, rows, feats), BF16)
    (lanes,) = call(lanes_kernel, [jax.ShapeDtypeStruct((8, LANES), F32)], flops=LANES_COST)
    keep, send, bundle, rates = call(
        start_kernel,
        [
            jax.ShapeDtypeStruct((rows, 5 * LANES), F32),
            payload_shape,
            jax.ShapeDtypeStruct((feats, 4 * LANES + feats), BF16),
            jax.ShapeDtypeStruct((8, LANES), F32),
        ],
        lanes, tok, norm_gain, floor_rate, head_gain, *weights, flops=10**8,
    )
    received = swap(send)
    (payload,) = call(pair_kernel, [payload_shape], lanes, keep, received, flops=10**6)
    bundle_b = swap(bundle)
    pieces = [w_output]
    for k in range(1, n_x):
        pieces.append(lax.ppermute(w_output, "x", [(i, (i + k) % n_x) for i in range(n_x)]))
    gathered = jnp.stack(pieces)
    w_out = (gathered, swap(gathered))

    terms = []
    for layer in range(2):
        arrived = spread(payload, "z")
        gated, term = call(
            functools.partial(mix_kernel, layer),
            [
                jax.ShapeDtypeStruct((n_x * n_z, own_rows, LANES), BF16),
                jax.ShapeDtypeStruct((3, own_rows, LANES), F32),
            ],
            arrived, rates, state, flops=10**7,
        )
        terms.append(term)
        heads = spread(gated, ("x", "z")).reshape(n_x, n_z, own_rows, LANES)
        (own,) = call(
            functools.partial(output_kernel, layer),
            [jax.ShapeDtypeStruct((rows, 2 * feats), BF16)],
            heads, *w_out, flops=10**8,
        )
        parts = [own]
        for k in range(1, n_y):
            parts.append(lax.ppermute(own, "y", [(i, i ^ k) for i in range(n_y)]))
        if layer == 0:
            payload, x = call(
                middle_kernel, [payload_shape, x_shape],
                *parts, lanes, tok, norm_gain, *weights, bundle_b, flops=10**8,
            )
    half = jax.ShapeDtypeStruct((rows, feats), BF16)
    keep, send = call(last_kernel, [half, half], *parts, x, flops=10**6)
    states = new_states(*terms, state)
    received = swap(send)
    (mixed,) = call(
        join_kernel, [jax.ShapeDtypeStruct((n_z, 2, own_rows, feats), BF16)],
        keep, received, flops=10**6,
    )
    return mixed.reshape(batch, feats), states


def solution(mesh):
    n_tp, n_dp = mesh.devices.shape
    fine = Mesh(mesh.devices.reshape(4, n_tp // 4, n_dp // 2, 2), ("y", "x", "z", "c"))
    dp, tp = ("z", "c"), ("y", "x")
    in_specs = (
        P(None, dp),
        P(None, dp),
        P(None, dp, tp),
        P(None, dp, tp),
        P(None, dp, tp),
        P(None, dp, tp),
        P(None, tp),
        P(),
        P(None, tp, dp),
        P(None, dp, tp, None, None),
    )
    out_specs = (P(None, dp), P(None, dp, tp, None, None))
    return jax.shard_map(
        per_device, mesh=fine, in_specs=in_specs, out_specs=out_specs, check_vma=False
    )
```

profile of v0, /device:TPU:1, one launch (start us, length us, event | category | flops | bytes accessed | tf_op | source)
XLA Modules:
  0.0 97.6 jit_solution(17709805372261699307)
XLA Ops:
  0.6 0.0 copy-start.8
  0.6 0.0 copy-start.6
  0.7 0.0 copy-start.4
  0.7 0.0 copy-start.2
  0.7 0.0 copy-start.11
  0.7 0.0 copy-start.13
  0.7 0.0 copy-start
  0.8 0.8 copy-done.8
  1.5 0.1 copy-done.6
  1.6 0.1 copy-done.4
  1.7 0.1 copy-done.2
  1.7 0.1 copy-done.1
  1.9 0.3 shard_map.114
  2.2 0.0 copy-start.14
  2.2 0.7 copy-done.14
  2.9 3.2 %collective-permute-start = (bf16[8,16,640]{2,1,0:T(8,128)(2,1)S(1)}, bf16[8,16,640]{2,1,0:T(8,128)(2,1)S(1)}, u32[]{:S(2)}, u32[]{:S(2)}) collective-permute-start(bf16[8,16,640]{2,1,0:T(8,128)(2,1)S(1)} %get-tuple-element.15), channel_id=1, source_target_pairs={{0,1},{1,0},{2,3},{3,2},{4,5},{5,4},{6,7},{7,6},{8,9},{9,8},{10,11... | collective-permute-start | bytes 491528 | tf_op jit(solution)/shard_map/ppermute | solution.py:245
  6.1 0.0 copy-done.15
  6.1 0.0 collective-permute-start.1
  6.1 2.7 %collective-permute-start.3 = (bf16[2,128,256]{2,1,0:T(8,128)(2,1)S(1)}, bf16[2,128,256]{2,1,0:T(8,128)(2,1)S(1)}, u32[]{:S(2)}, u32[]{:S(2)}) collective-permute-start(bf16[2,128,256]{2,1,0:T(8,128)(2,1)S(1)} %copy-done.15), channel_id=1, source_target_pairs={{0,48},{16,0},{32,16},{48,32},{1,49},{17,1},{33,17},{49,33},{2,50}... | collective-permute-start | bytes 393224 | tf_op jit(solution)/shard_map/ppermute | solution.py:267
  8.8 0.0 collective-permute-start.2
  8.8 0.0 collective-permute-done.received
  8.8 0.9 shard_map.115
  9.7 8.0 %all-to-all-start = ((bf16[8,16,640]{2,1,0:T(8,128)(2,1)}), bf16[8,16,640]{2,1,0:T(8,128)(2,1)S(1)}, u32[]{:S(2)}, u32[]{:S(2)}) async-start(bf16[8,16,640]{2,1,0:T(8,128)(2,1)} %shard_map.115), calls=%async_computation | async-start | bytes 327680 | tf_op jit(solution)/shard_map/all_to_all | solution.py:233
  17.7 0.0 collective-permute-done.1
  17.7 0.0 collective-permute-done.3
  17.7 0.0 collective-permute-done.2
  17.7 0.1 pad_maximum_fusion.w_a
  17.8 1.2 %collective-permute-start.4 = (bf16[4,2,128,256]{3,2,1,0:T(8,128)(2,1)S(1)}, bf16[4,2,128,256]{3,2,1,0:T(8,128)(2,1)S(1)}, u32[]{:S(2)}, u32[]{:S(2)}) collective-permute-start(bf16[4,2,128,256]{3,2,1,0:T(8,128)(2,1)S(1)} %pad_maximum_fusion.w_a), channel_id=1, source_target_pairs={{0,1},{1,0},{2,3},{3,2},{4,5},{5,4},{6,7},{7,6},{8,9},{9,8},{10,11... | collective-permute-start | bytes 1572872 | tf_op jit(solution)/shard_map/ppermute | solution.py:245
  19.0 6.7 %all-to-all-done.arrived = bf16[8,16,640]{2,1,0:T(8,128)(2,1)S(1)} async-done(((bf16[8,16,640]{2,1,0:T(8,128)(2,1)}), bf16[8,16,640]{2,1,0:T(8,128)(2,1)S(1)}, u32[]{:S(2)}, u32[]{:S(2)}) %all-to-all-start) | async-done | bytes 163872 | tf_op jit(solution)/shard_map/all_to_all | solution.py:233
  25.8 0.7 shard_map.116
  26.5 0.0 copy-start.10
  26.5 0.6 copy-done.10
  27.2 4.2 %all-to-all-start.1 = ((bf16[32,16,128]{2,1,0:T(8,128)(2,1)}), bf16[32,16,128]{2,1,0:T(8,128)(2,1)S(1)}, u32[]{:S(2)}, u32[]{:S(2)}) async-start(bf16[32,16,128]{2,1,0:T(8,128)(2,1)} %copy-done.10), calls=%async_computation.1 | async-start | bytes 262144 | tf_op jit(solution)/shard_map/all_to_all | solution.py:233
  31.3 2.4 %collective-permute-start.8 = (bf16[256,768]{1,0:T(8,128)(2,1)}, bf16[256,768]{1,0:T(8,128)(2,1)}, u32[]{:S(2)}, u32[]{:S(2)}) collective-permute-start(bf16[256,768]{1,0:T(8,128)(2,1)} %copy-done.14), channel_id=1, source_target_pairs={{0,1},{1,0},{2,3},{3,2},{4,5},{5,4},{6,7},{7,6},{8,9},{9,8},{10,11... | collective-permute-start | bytes 1179656 | tf_op jit(solution)/shard_map/ppermute | solution.py:245
  33.8 0.0 collective-permute-done.4.w_b
  33.8 6.7 %all-to-all-done.1 = bf16[32,16,128]{2,1,0:T(8,128)(2,1)S(1)} async-done(((bf16[32,16,128]{2,1,0:T(8,128)(2,1)}), bf16[32,16,128]{2,1,0:T(8,128)(2,1)S(1)}, u32[]{:S(2)}, u32[]{:S(2)}) %all-to-all-start.1) | async-done | bytes 131104 | tf_op jit(solution)/shard_map/all_to_all | solution.py:233
  40.5 0.3 shard_map.117.p0
  40.8 2.8 %collective-permute-start.7 = (bf16[128,512]{1,0:T(8,128)(2,1)S(1)}, bf16[128,512]{1,0:T(8,128)(2,1)S(1)}, u32[]{:S(2)}, u32[]{:S(2)}) collective-permute-start(bf16[128,512]{1,0:T(8,128)(2,1)S(1)} %shard_map.117.p0), channel_id=1, source_target_pairs={{0,192},{64,128},{128,64},{192,0},{1,193},{65,129},{129,65},{193,1... | collective-permute-start | bytes 393224 | tf_op jit(solution)/shard_map/ppermute | solution.py:291
  43.6 0.4 collective-permute-start.6
  44.0 0.3 collective-permute-start.5
  44.3 0.0 collective-permute-done.8.refs_4_
  44.3 2.6 %collective-permute-done.7.p3 = bf16[128,512]{1,0:T(8,128)(2,1)S(1)} collective-permute-done((bf16[128,512]{1,0:T(8,128)(2,1)S(1)}, bf16[128,512]{1,0:T(8,128)(2,1)S(1)}, u32[]{:S(2)}, u32[]{:S(2)}) %collective-permute-start.7) | collective-permute-done | bytes 131104 | tf_op jit(solution)/shard_map/ppermute | solution.py:291
  46.9 2.0 %collective-permute-done.6.p2 = bf16[128,512]{1,0:T(8,128)(2,1)S(1)} collective-permute-done((bf16[128,512]{1,0:T(8,128)(2,1)S(1)}, bf16[128,512]{1,0:T(8,128)(2,1)S(1)}, u32[]{:S(2)}, u32[]{:S(2)}) %collective-permute-start.6) | collective-permute-done | bytes 131104 | tf_op jit(solution)/shard_map/ppermute | solution.py:291
  49.0 0.0 collective-permute-done.5.p1
  49.0 0.9 copy-done.3
  49.9 0.9 copy-done.5
  50.8 0.9 copy-done.7
  51.7 0.9 copy-done.9
  52.6 1.3 %shard_map.118 = (bf16[8,16,640]{2,1,0:T(8,128)(2,1)S(1)}, bf16[2,128,256]{2,1,0:T(8,128)(2,1)S(1)}) custom-call(bf16[128,512]{1,0:T(8,128)(2,1)S(1)} %shard_map.117.p0, bf16[128,512]{1,0:T(8,128)(2,1)S(1)} %collective-permute-done.5.p1, bf16[128,512]{1,0:T(8,128)(2,1)S(1)} %collective-permute-done.6.p2, bf16[128,512]{1,0:T(8,128)(2,1)S(1)} %collective-permute-done.7.p3, ...), custom_call_target="tpu_custom_call" | custom-call | flops 100000000 | bytes 1579008 | tf_op jit(solution)/shard_map/pallas_call | solution.py:25
  53.9 10.7 %all_to_all.20.arrived = bf16[8,16,640]{2,1,0:T(8,128)(2,1)S(1)} all-to-all(bf16[8,16,640]{2,1,0:T(8,128)(2,1)S(1)} %get-tuple-element.19), channel_id=1, replica_groups=mesh['y'=4,'x'=4,'z'=8,'c'=2] {'z'}, dimensions={0} | all-to-all | bytes 327680 | tf_op jit(solution)/shard_map/all_to_all | solution.py:233
  64.6 0.7 shard_map.119
  65.3 12.1 %all_to_all.21 = bf16[32,16,128]{2,1,0:T(8,128)(2,1)S(1)} all-to-all(bf16[32,16,128]{2,1,0:T(8,128)(2,1)S(1)} %get-tuple-element.20), channel_id=1, replica_groups=mesh['y'=4,'x'=4,'z'=8,'c'=2] {'x','z'}, dimensions={0} | all-to-all | bytes 262144 | tf_op jit(solution)/shard_map/all_to_all | solution.py:233
  77.4 0.3 shard_map.120.refs_0_
  77.7 1.7 %collective-permute-start.11 = (bf16[128,512]{1,0:T(8,128)(2,1)S(1)}, bf16[128,512]{1,0:T(8,128)(2,1)S(1)}, u32[]{:S(2)}, u32[]{:S(2)}) collective-permute-start(bf16[128,512]{1,0:T(8,128)(2,1)S(1)} %shard_map.120.refs_0_), channel_id=1, source_target_pairs={{0,192},{64,128},{128,64},{192,0},{1,193},{65,129},{129,65},{193,1... | collective-permute-start | bytes 393224 | tf_op jit(solution)/shard_map/ppermute | solution.py:291
  79.5 0.7 collective-permute-start.10
  80.1 0.9 collective-permute-start.9
  81.1 2.1 %collective-permute-done.11.refs_3_ = bf16[128,512]{1,0:T(8,128)(2,1)S(1)} collective-permute-done((bf16[128,512]{1,0:T(8,128)(2,1)S(1)}, bf16[128,512]{1,0:T(8,128)(2,1)S(1)}, u32[]{:S(2)}, u32[]{:S(2)}) %collective-permute-start.11) | collective-permute-done | bytes 131104 | tf_op jit(solution)/shard_map/ppermute | solution.py:291
  83.1 1.6 %collective-permute-done.10.refs_2_ = bf16[128,512]{1,0:T(8,128)(2,1)S(1)} collective-permute-done((bf16[128,512]{1,0:T(8,128)(2,1)S(1)}, bf16[128,512]{1,0:T(8,128)(2,1)S(1)}, u32[]{:S(2)}, u32[]{:S(2)}) %collective-permute-start.10) | collective-permute-done | bytes 131104 | tf_op jit(solution)/shard_map/ppermute | solution.py:291
  84.8 0.1 collective-permute-done.9.refs_1_
  84.9 0.1 shard_map.121
  85.0 8.8 %collective-permute-start.12 = (bf16[128,256]{1,0:T(8,128)(2,1)S(1)}, bf16[128,256]{1,0:T(8,128)(2,1)S(1)}, u32[]{:S(2)}, u32[]{:S(2)}) collective-permute-start(bf16[128,256]{1,0:T(8,128)(2,1)S(1)} %get-tuple-element.23), channel_id=1, source_target_pairs={{0,1},{1,0},{2,3},{3,2},{4,5},{5,4},{6,7},{7,6},{8,9},{9,8},{10,11... | collective-permute-start | bytes 196616 | tf_op jit(solution)/shard_map/ppermute | solution.py:245
  93.8 3.2 %new_states.1 = f32[2,16,1,128,128]{4,3,2,1,0:T(8,128)} custom-call(f32[3,16,128]{2,1,0:T(8,128)S(1)} %get-tuple-element.24.terms_a, f32[3,16,128]{2,1,0:T(8,128)S(1)} %get-tuple-element.25.terms_b, f32[2,16,1,128,128]{4,3,2,1,0:T(8,128)S(1)} %copy-done), custom_call_target="tpu_custom_call" | custom-call | flops 10000000 | bytes 4194304 | tf_op jit(solution)/shard_map/new_states/pallas_call | solution.py:203
  96.9 0.0 collective-permute-done.12.received
  96.9 0.7 shard_map.122
  (12 shorter events, 0.0 us)
Async XLA Ops:
  0.6 0.9 copy-start.8
  0.6 1.0 copy-start.6
  0.7 1.0 %copy-start.4 = (bf16[2,256,128]{2,1,0:T(8,128)(2,1)S(1)}, bf16[2,256,128]{2,1,0:T(8,128)(2,1)}, u32[]{:S(2)}) copy-start(bf16[2,256,128]{2,1,0:T(8,128)(2,1)} %refs_1_.3) | copy-start | bytes 393220
  0.7 1.1 %copy-start.2 = (bf16[2,256,128]{2,1,0:T(8,128)(2,1)S(1)}, bf16[2,256,128]{2,1,0:T(8,128)(2,1)}, u32[]{:S(2)}) copy-start(bf16[2,256,128]{2,1,0:T(8,128)(2,1)} %refs_0_.3) | copy-start | bytes 393220
  0.7 1.1 %copy-start.11 = (f32[2,256]{1,0:T(2,128)S(1)}, f32[2,256]{1,0:T(2,128)}, u32[]{:S(2)}) copy-start(f32[2,256]{1,0:T(2,128)} %gain.3) | copy-start | bytes 6148
  0.7 1.1 %copy-start.13 = (f32[2,128]{1,0:T(2,128)S(1)}, f32[2,128]{1,0:T(2,128)}, u32[]{:S(2)}) copy-start(f32[2,128]{1,0:T(2,128)} %head_gain.1) | copy-start | bytes 3076
  0.7 1.0 %copy-start.12 = (f32[2,128]{1,0:T(2,128)S(1)}, f32[2,128]{1,0:T(2,128)}, u32[]{:S(2)}) copy-start(f32[2,128]{1,0:T(2,128)} %floor_rate.1) | copy-start | bytes 3076
  0.7 1.2 %copy-start.1 = (bf16[256,256]{1,0:T(8,128)(2,1)S(1)}, bf16[256,256]{1,0:T(8,128)(2,1)}, u32[]{:S(2)}) copy-start(bf16[256,256]{1,0:T(8,128)(2,1)} %param.10) | copy-start | bytes 393220
  0.7 5.4 %copy-start.15 = (bf16[2,128,256]{2,1,0:T(8,128)(2,1)S(1)}, bf16[2,128,256]{2,1,0:T(8,128)(2,1)}, u32[]{:S(2)}) copy-start(bf16[2,128,256]{2,1,0:T(8,128)(2,1)} %param.18) | copy-start | bytes 393220
  0.7 25.0 %copy-start = (f32[2,16,1,128,128]{4,3,2,1,0:T(8,128)S(1)}, f32[2,16,1,128,128]{4,3,2,1,0:T(8,128)}, u32[]{:S(2)}) copy-start(f32[2,16,1,128,128]{4,3,2,1,0:T(8,128)} %state.5) | copy-start | bytes 6291460
  2.2 0.7 copy-start.14
  2.9 5.9 %collective-permute-start = (bf16[8,16,640]{2,1,0:T(8,128)(2,1)S(1)}, bf16[8,16,640]{2,1,0:T(8,128)(2,1)S(1)}, u32[]{:S(2)}, u32[]{:S(2)}) collective-permute-start(bf16[8,16,640]{2,1,0:T(8,128)(2,1)S(1)} %get-tuple-element.15), channel_id=1, source_target_pairs={{0,1},{1,0},{2,3},{3,2},{4,5},{5,4},{6,7},{7,6},{8,9},{9,8},{10,11... | collective-permute-start | bytes 491528 | tf_op jit(solution)/shard_map/ppermute | solution.py:245
  6.1 11.5 %collective-permute-start.1 = (bf16[2,128,256]{2,1,0:T(8,128)(2,1)S(1)}, bf16[2,128,256]{2,1,0:T(8,128)(2,1)S(1)}, u32[]{:S(2)}, u32[]{:S(2)}) collective-permute-start(bf16[2,128,256]{2,1,0:T(8,128)(2,1)S(1)} %copy-done.15), channel_id=1, source_target_pairs={{0,16},{16,32},{32,48},{48,0},{1,17},{17,33},{33,49},{49,1},{2,18}... | collective-permute-start | bytes 393224 | tf_op jit(solution)/shard_map/ppermute | solution.py:267
  6.1 11.6 %collective-permute-start.3 = (bf16[2,128,256]{2,1,0:T(8,128)(2,1)S(1)}, bf16[2,128,256]{2,1,0:T(8,128)(2,1)S(1)}, u32[]{:S(2)}, u32[]{:S(2)}) collective-permute-start(bf16[2,128,256]{2,1,0:T(8,128)(2,1)S(1)} %copy-done.15), channel_id=1, source_target_pairs={{0,48},{16,0},{32,16},{48,32},{1,49},{17,1},{33,17},{49,33},{2,50}... | collective-permute-start | bytes 393224 | tf_op jit(solution)/shard_map/ppermute | solution.py:267
  8.8 8.9 %collective-permute-start.2 = (bf16[2,128,256]{2,1,0:T(8,128)(2,1)S(1)}, bf16[2,128,256]{2,1,0:T(8,128)(2,1)S(1)}, u32[]{:S(2)}, u32[]{:S(2)}) collective-permute-start(bf16[2,128,256]{2,1,0:T(8,128)(2,1)S(1)} %copy-done.15), channel_id=1, source_target_pairs={{0,32},{16,48},{32,0},{48,16},{1,33},{17,49},{33,1},{49,17},{2,34}... | collective-permute-start | bytes 393224 | tf_op jit(solution)/shard_map/ppermute | solution.py:267
  9.7 16.1 %all-to-all-start = ((bf16[8,16,640]{2,1,0:T(8,128)(2,1)}), bf16[8,16,640]{2,1,0:T(8,128)(2,1)S(1)}, u32[]{:S(2)}, u32[]{:S(2)}) async-start(bf16[8,16,640]{2,1,0:T(8,128)(2,1)} %shard_map.115), calls=%async_computation | async-start | bytes 327680 | tf_op jit(solution)/shard_map/all_to_all | solution.py:233
  17.8 16.0 %collective-permute-start.4 = (bf16[4,2,128,256]{3,2,1,0:T(8,128)(2,1)S(1)}, bf16[4,2,128,256]{3,2,1,0:T(8,128)(2,1)S(1)}, u32[]{:S(2)}, u32[]{:S(2)}) collective-permute-start(bf16[4,2,128,256]{3,2,1,0:T(8,128)(2,1)S(1)} %pad_maximum_fusion.w_a), channel_id=1, source_target_pairs={{0,1},{1,0},{2,3},{3,2},{4,5},{5,4},{6,7},{7,6},{8,9},{9,8},{10,11... | collective-permute-start | bytes 1572872 | tf_op jit(solution)/shard_map/ppermute | solution.py:245
  26.5 0.7 copy-start.10
  27.2 13.3 %all-to-all-start.1 = ((bf16[32,16,128]{2,1,0:T(8,128)(2,1)}), bf16[32,16,128]{2,1,0:T(8,128)(2,1)S(1)}, u32[]{:S(2)}, u32[]{:S(2)}) async-start(bf16[32,16,128]{2,1,0:T(8,128)(2,1)} %copy-done.10), calls=%async_computation.1 | async-start | bytes 262144 | tf_op jit(solution)/shard_map/all_to_all | solution.py:233
  31.3 13.0 %collective-permute-start.8 = (bf16[256,768]{1,0:T(8,128)(2,1)}, bf16[256,768]{1,0:T(8,128)(2,1)}, u32[]{:S(2)}, u32[]{:S(2)}) collective-permute-start(bf16[256,768]{1,0:T(8,128)(2,1)} %copy-done.14), channel_id=1, source_target_pairs={{0,1},{1,0},{2,3},{3,2},{4,5},{5,4},{6,7},{7,6},{8,9},{9,8},{10,11... | collective-permute-start | bytes 1179656 | tf_op jit(solution)/shard_map/ppermute | solution.py:245
  40.8 6.1 %collective-permute-start.7 = (bf16[128,512]{1,0:T(8,128)(2,1)S(1)}, bf16[128,512]{1,0:T(8,128)(2,1)S(1)}, u32[]{:S(2)}, u32[]{:S(2)}) collective-permute-start(bf16[128,512]{1,0:T(8,128)(2,1)S(1)} %shard_map.117.p0), channel_id=1, source_target_pairs={{0,192},{64,128},{128,64},{192,0},{1,193},{65,129},{129,65},{193,1... | collective-permute-start | bytes 393224 | tf_op jit(solution)/shard_map/ppermute | solution.py:291
  43.6 5.4 %collective-permute-start.6 = (bf16[128,512]{1,0:T(8,128)(2,1)S(1)}, bf16[128,512]{1,0:T(8,128)(2,1)S(1)}, u32[]{:S(2)}, u32[]{:S(2)}) collective-permute-start(bf16[128,512]{1,0:T(8,128)(2,1)S(1)} %shard_map.117.p0), channel_id=1, source_target_pairs={{0,128},{64,192},{128,0},{192,64},{1,129},{65,193},{129,1},{193,65... | collective-permute-start | bytes 393224 | tf_op jit(solution)/shard_map/ppermute | solution.py:291
  44.0 5.0 %collective-permute-start.5 = (bf16[128,512]{1,0:T(8,128)(2,1)S(1)}, bf16[128,512]{1,0:T(8,128)(2,1)S(1)}, u32[]{:S(2)}, u32[]{:S(2)}) collective-permute-start(bf16[128,512]{1,0:T(8,128)(2,1)S(1)} %shard_map.117.p0), channel_id=1, source_target_pairs={{0,64},{64,0},{128,192},{192,128},{1,65},{65,1},{129,193},{193,129... | collective-permute-start | bytes 393224 | tf_op jit(solution)/shard_map/ppermute | solution.py:291
  49.0 0.9 copy-start.3
  49.9 0.9 copy-start.5
  50.8 0.9 copy-start.7
  51.7 0.9 copy-start.9
  77.7 5.4 %collective-permute-start.11 = (bf16[128,512]{1,0:T(8,128)(2,1)S(1)}, bf16[128,512]{1,0:T(8,128)(2,1)S(1)}, u32[]{:S(2)}, u32[]{:S(2)}) collective-permute-start(bf16[128,512]{1,0:T(8,128)(2,1)S(1)} %shard_map.120.refs_0_), channel_id=1, source_target_pairs={{0,192},{64,128},{128,64},{192,0},{1,193},{65,129},{129,65},{193,1... | collective-permute-start | bytes 393224 | tf_op jit(solution)/shard_map/ppermute | solution.py:291
  79.5 5.3 %collective-permute-start.10 = (bf16[128,512]{1,0:T(8,128)(2,1)S(1)}, bf16[128,512]{1,0:T(8,128)(2,1)S(1)}, u32[]{:S(2)}, u32[]{:S(2)}) collective-permute-start(bf16[128,512]{1,0:T(8,128)(2,1)S(1)} %shard_map.120.refs_0_), channel_id=1, source_target_pairs={{0,128},{64,192},{128,0},{192,64},{1,129},{65,193},{129,1},{193,65... | collective-permute-start | bytes 393224 | tf_op jit(solution)/shard_map/ppermute | solution.py:291
  80.1 4.7 %collective-permute-start.9 = (bf16[128,512]{1,0:T(8,128)(2,1)S(1)}, bf16[128,512]{1,0:T(8,128)(2,1)S(1)}, u32[]{:S(2)}, u32[]{:S(2)}) collective-permute-start(bf16[128,512]{1,0:T(8,128)(2,1)S(1)} %shard_map.120.refs_0_), channel_id=1, source_target_pairs={{0,64},{64,0},{128,192},{192,128},{1,65},{65,1},{129,193},{193,129... | collective-permute-start | bytes 393224 | tf_op jit(solution)/shard_map/ppermute | solution.py:291
  85.0 12.0 %collective-permute-start.12 = (bf16[128,256]{1,0:T(8,128)(2,1)S(1)}, bf16[128,256]{1,0:T(8,128)(2,1)S(1)}, u32[]{:S(2)}, u32[]{:S(2)}) collective-permute-start(bf16[128,256]{1,0:T(8,128)(2,1)S(1)} %get-tuple-element.23), channel_id=1, source_target_pairs={{0,1},{1,0},{2,3},{3,2},{4,5},{5,4},{6,7},{7,6},{8,9},{9,8},{10,11... | collective-permute-start | bytes 196616 | tf_op jit(solution)/shard_map/ppermute | solution.py:245
where the time goes:
time: 98 us; the launch traced here: 97.6 us
  starting transfers between devices  37.3 us (38%)
  blocking collectives  22.8 us (23%)
  waiting for transfers between devices  21.9 us (22%)
  Pallas kernels  8.47 us (9%)
  local copies, waits for them, and re-layouts  6.15 us (6%)
    all_to_all x2, blocking collectives, spread(): return lax.all_to_all(copies, axes, split_axis=0, concat_axis=0, tiled=True)  22.8 us
    ppermute x4, starting transfers between devices, swap(): return lax.ppermute(v, 'c', [(0, 1), (1, 0)])  15.7 us
    all_to_all x2, waiting for transfers between devices, spread(): return lax.all_to_all(copies, axes, split_axis=0, concat_axis=0, tiled=True)  13.5 us
    all_to_all x2, starting transfers between devices, spread(): return lax.all_to_all(copies, axes, split_axis=0, concat_axis=0, tiled=True)  12.2 us
    ppermute x6, waiting for transfers between devices, per_device(): parts.append(lax.ppermute(own, 'y', [(i, i ^ k) for i in range(n_y)]))  8.46 us
    ppermute x6, starting transfers between devices, per_device(): parts.append(lax.ppermute(own, 'y', [(i, i ^ k) for i in range(n_y)]))  6.83 us
    unnamed x32, local copies, waits for them, and re-layouts  6.15 us
    pallas_call x10, Pallas kernels, call(): pl.pallas_call(kernel, out_shape=outs, in_specs=[vmem] * len(args), out_s...  5.3 us
  transfers between devices with their start and end apart: 15, of which 7 were waited for; matrix products, arithmetic and copies ran while one was open for 0% of the time, Pallas kernels for 5%

commit v1 on v0

--- a/solution.py
+++ b/solution.py
@@ -212,21 +212,19 @@
     )(terms_a, terms_b, state)
 
 
-def output_kernel(layer, heads, w_a, w_b, out_ref):
+def output_kernel(layer, heads, *refs):
+    pieces, out_ref = refs[:-1], refs[-1]
     my_x = lax.axis_index("x")
     n_x = heads.shape[0]
     rows = heads.shape[1] * heads.shape[2]
-    for half, w in enumerate((w_a, w_b)):
+    feats = pieces[0].shape[3]
+    for half in range(2):
         total = None
-        for i in range(n_x):
-            block = w[lax.rem(my_x - i + n_x, n_x), layer]
-            product = jnp.dot(
-                heads[i].reshape(rows, LANES), block, preferred_element_type=F32
-            )
+        for k in range(n_x):
+            head = heads[lax.rem(my_x - k + n_x, n_x)].reshape(rows, LANES)
+            product = jnp.dot(head, pieces[k][half, layer], preferred_element_type=F32)
             total = product if total is None else total + product
-        total = total.astype(BF16)
-        feats = total.shape[1]
-        out_ref[:, half * feats : (half + 1) * feats] = total
+        out_ref[:, half * feats : (half + 1) * feats] = total.astype(BF16)
 
 
 def spread(copies, axes):
@@ -262,11 +260,11 @@
     received = swap(send)
     (payload,) = call(pair_kernel, [payload_shape], lanes, keep, received, flops=10**6)
     bundle_b = swap(bundle)
-    pieces = [w_output]
+    w_other = swap(w_output)
+    both = jnp.stack([w_output, w_other])
+    w_out = [both]
     for k in range(1, n_x):
-        pieces.append(lax.ppermute(w_output, "x", [(i, (i + k) % n_x) for i in range(n_x)]))
-    gathered = jnp.stack(pieces)
-    w_out = (gathered, swap(gathered))
+        w_out.append(lax.ppermute(both, "x", [(i, (i + k) % n_x) for i in range(n_x)]))
 
     terms = []
     for layer in range(2):

time: 98 us -> 96.2 us (0.982)
  starting transfers between devices: 37.3 us -> 35.9 us
    all_to_all x2, waiting for transfers between devices: 13.5 us -> 8.62 us  [spread(): return lax.all_to_all(copies, axes, split_axis=0, concat_axis=0, tiled=True)]
    ppermute x4, starting transfers between devices: 15.7 us -> 13.1 us  [swap(): return lax.ppermute(v, 'c', [(0, 1), (1, 0)])]
    ppermute x3, waiting for transfers between devices: 0.01 us -> 2.22 us  [per_device(): lax.ppermute(both, 'x', [(i, (i + k) % n_x) for i in range(n_x)])]
    ppermute x4, waiting for transfers between devices: 0.01 us -> 2.02 us  [swap(): return lax.ppermute(v, 'c', [(0, 1), (1, 0)])]
    ppermute x3, starting transfers between devices: 2.68 us -> 3.67 us  [per_device(): lax.ppermute(both, 'x', [(i, (i + k) % n_x) for i in range(n_x)])]
  transfers between devices with their start and end apart: 15 -> 15, of which waited for: 7 -> 9; matrix products, arithmetic and copies ran while one was open for 0% -> 0% of each run, Pallas kernels for 5% -> 4%
where the time goes in v1:
time: 96.2 us; the launch traced here: 95.8 us
  starting transfers between devices  35.9 us (37%)
  blocking collectives  22.8 us (24%)
  waiting for transfers between devices  21.6 us (22%)
  Pallas kernels  8.48 us (9%)
  local copies, waits for them, and re-layouts  6.15 us (6%)
    all_to_all x2, blocking collectives, spread(): return lax.all_to_all(copies, axes, split_axis=0, concat_axis=0, tiled=True)  22.8 us
    ppermute x4, starting transfers between devices, swap(): return lax.ppermute(v, 'c', [(0, 1), (1, 0)])  13.1 us
    all_to_all x2, starting transfers between devices, spread(): return lax.all_to_all(copies, axes, split_axis=0, concat_axis=0, tiled=True)  12.3 us
    ppermute x6, waiting for transfers between devices, per_device(): parts.append(lax.ppermute(own, 'y', [(i, i ^ k) for i in range(n_y)]))  8.73 us
    all_to_all x2, waiting for transfers between devices, spread(): return lax.all_to_all(copies, axes, split_axis=0, concat_axis=0, tiled=True)  8.62 us
    ppermute x6, starting transfers between devices, per_device(): parts.append(lax.ppermute(own, 'y', [(i, i ^ k) for i in range(n_y)]))  6.85 us
    unnamed x32, local copies, waits for them, and re-layouts  6.15 us
    pallas_call x10, Pallas kernels, call(): pl.pallas_call(kernel, out_shape=outs, in_specs=[vmem] * len(args), out_s...  5.31 us
  transfers between devices with their start and end apart: 15, of which 9 were waited for; matrix products, arithmetic and copies ran while one was open for 0% of the time, Pallas kernels for 4%

profile of v1, /device:TPU:1, one launch (start us, length us, event | category | flops | bytes accessed | tf_op | source)
XLA Modules:
  0.0 95.8 jit_solution(3402621151132095650)
XLA Ops:
  0.6 0.0 copy-start.8
  0.6 0.0 copy-start.6
  0.7 0.0 copy-start.4
  0.7 0.0 copy-start.2
  0.7 0.0 copy-start.11
  0.7 0.0 copy-start.13
  0.7 0.0 copy-start.12
  0.7 0.0 copy-start.1
  0.7 0.0 copy-start
  0.8 0.8 copy-done.8
  1.5 0.1 copy-done.6
  1.6 0.1 copy-done.4
  1.7 0.1 copy-done.2
  1.7 0.1 copy-done.1
  1.9 0.3 shard_map.114
  2.2 0.0 copy-start.14
  2.2 0.7 copy-done.14
  2.9 3.2 %collective-permute-start = (bf16[8,16,640]{2,1,0:T(8,128)(2,1)S(1)}, bf16[8,16,640]{2,1,0:T(8,128)(2,1)S(1)}, u32[]{:S(2)}, u32[]{:S(2)}) collective-permute-start(bf16[8,16,640]{2,1,0:T(8,128)(2,1)S(1)} %get-tuple-element.15), channel_id=1, source_target_pairs={{0,1},{1,0},{2,3},{3,2},{4,5},{5,4},{6,7},{7,6},{8,9},{9,8},{10,11... | collective-permute-start | bytes 491528 | tf_op jit(solution)/shard_map/ppermute | solution.py:243
  6.1 1.0 %collective-permute-done.received = bf16[8,16,640]{2,1,0:T(8,128)(2,1)S(1)} collective-permute-done((bf16[8,16,640]{2,1,0:T(8,128)(2,1)S(1)}, bf16[8,16,640]{2,1,0:T(8,128)(2,1)S(1)}, u32[]{:S(2)}, u32[]{:S(2)}) %collective-permute-start) | collective-permute-done | bytes 163872 | tf_op jit(solution)/shard_map/ppermute | solution.py:243
  7.2 0.9 shard_map.115
  8.0 6.5 %all-to-all-start = ((bf16[8,16,640]{2,1,0:T(8,128)(2,1)}), bf16[8,16,640]{2,1,0:T(8,128)(2,1)S(1)}, u32[]{:S(2)}, u32[]{:S(2)}) async-start(bf16[8,16,640]{2,1,0:T(8,128)(2,1)} %shard_map.115), calls=%async_computation | async-start | bytes 327680 | tf_op jit(solution)/shard_map/all_to_all | solution.py:231
  14.5 0.7 collective-permute-start.1
  15.3 1.0 %collective-permute-done.1 = bf16[2,128,256]{2,1,0:T(8,128)(2,1)S(1)} collective-permute-done((bf16[2,128,256]{2,1,0:T(8,128)(2,1)S(1)}, bf16[2,128,256]{2,1,0:T(8,128)(2,1)S(1)}, u32[]{:S(2)}, u32[]{:S(2)}) %collective-permute-start.1) | collective-permute-done | bytes 131104 | tf_op jit(solution)/shard_map/ppermute | solution.py:243
  16.3 2.6 %collective-permute-start.4 = (bf16[2,2,128,256]{3,2,1,0:T(8,128)(2,1)S(1)}, bf16[2,2,128,256]{3,2,1,0:T(8,128)(2,1)S(1)}, u32[]{:S(2)}, u32[]{:S(2)}) collective-permute-start(bf16[2,2,128,256]{3,2,1,0:T(8,128)(2,1)S(1)} %pad_maximum_fusion.refs_0_), channel_id=1, source_target_pairs={{0,48},{16,0},{32,16},{48,32},{1,49},{17,1},{33,17},{49,33},{2,50}... | collective-permute-start | bytes 786440 | tf_op jit(solution)/shard_map/ppermute | solution.py:267
  18.8 0.5 collective-permute-start.3
  19.3 0.6 collective-permute-start.2
  19.9 3.2 %all-to-all-done.arrived = bf16[8,16,640]{2,1,0:T(8,128)(2,1)S(1)} async-done(((bf16[8,16,640]{2,1,0:T(8,128)(2,1)}), bf16[8,16,640]{2,1,0:T(8,128)(2,1)S(1)}, u32[]{:S(2)}, u32[]{:S(2)}) %all-to-all-start) | async-done | bytes 163872 | tf_op jit(solution)/shard_map/all_to_all | solution.py:231
  23.2 0.7 shard_map.116
  23.9 0.0 copy-start.10
  23.9 0.6 copy-done.10
  24.6 5.8 %all-to-all-start.1 = ((bf16[32,16,128]{2,1,0:T(8,128)(2,1)}), bf16[32,16,128]{2,1,0:T(8,128)(2,1)S(1)}, u32[]{:S(2)}, u32[]{:S(2)}) async-start(bf16[32,16,128]{2,1,0:T(8,128)(2,1)} %copy-done.10), calls=%async_computation.1 | async-start | bytes 262144 | tf_op jit(solution)/shard_map/all_to_all | solution.py:231
  30.4 1.6 %collective-permute-start.8 = (bf16[256,768]{1,0:T(8,128)(2,1)}, bf16[256,768]{1,0:T(8,128)(2,1)}, u32[]{:S(2)}, u32[]{:S(2)}) collective-permute-start(bf16[256,768]{1,0:T(8,128)(2,1)} %copy-done.14), channel_id=1, source_target_pairs={{0,1},{1,0},{2,3},{3,2},{4,5},{5,4},{6,7},{7,6},{8,9},{9,8},{10,11... | collective-permute-start | bytes 1179656 | tf_op jit(solution)/shard_map/ppermute | solution.py:243
  32.0 0.0 collective-permute-done.4.refs_3_
  32.0 0.0 collective-permute-done.3.refs_2_
  32.0 2.2 %collective-permute-done.2.refs_1_ = bf16[2,2,128,256]{3,2,1,0:T(8,128)(2,1)S(1)} collective-permute-done((bf16[2,2,128,256]{3,2,1,0:T(8,128)(2,1)S(1)}, bf16[2,2,128,256]{3,2,1,0:T(8,128)(2,1)S(1)}, u32[]{:S(2)}, u32[]{:S(2)}) %collective-permute-start.2) | collective-permute-done | bytes 262176 | tf_op jit(solution)/shard_map/ppermute | solution.py:267
  34.2 5.4 %all-to-all-done.1 = bf16[32,16,128]{2,1,0:T(8,128)(2,1)S(1)} async-done(((bf16[32,16,128]{2,1,0:T(8,128)(2,1)}), bf16[32,16,128]{2,1,0:T(8,128)(2,1)S(1)}, u32[]{:S(2)}, u32[]{:S(2)}) %all-to-all-start.1) | async-done | bytes 131104 | tf_op jit(solution)/shard_map/all_to_all | solution.py:231
  39.6 0.3 shard_map.117.p0
  39.8 2.8 %collective-permute-start.7 = (bf16[128,512]{1,0:T(8,128)(2,1)S(1)}, bf16[128,512]{1,0:T(8,128)(2,1)S(1)}, u32[]{:S(2)}, u32[]{:S(2)}) collective-permute-start(bf16[128,512]{1,0:T(8,128)(2,1)S(1)} %shard_map.117.p0), channel_id=1, source_target_pairs={{0,192},{64,128},{128,64},{192,0},{1,193},{65,129},{129,65},{193,1... | collective-permute-start | bytes 393224 | tf_op jit(solution)/shard_map/ppermute | solution.py:289
  42.7 0.4 collective-permute-start.6
  43.0 0.3 collective-permute-start.5
  43.4 0.0 collective-permute-done.8.refs_4_
  43.4 2.6 %collective-permute-done.7.p3 = bf16[128,512]{1,0:T(8,128)(2,1)S(1)} collective-permute-done((bf16[128,512]{1,0:T(8,128)(2,1)S(1)}, bf16[128,512]{1,0:T(8,128)(2,1)S(1)}, u32[]{:S(2)}, u32[]{:S(2)}) %collective-permute-start.7) | collective-permute-done | bytes 131104 | tf_op jit(solution)/shard_map/ppermute | solution.py:289
  46.0 2.1 %collective-permute-done.6.p2 = bf16[128,512]{1,0:T(8,128)(2,1)S(1)} collective-permute-done((bf16[128,512]{1,0:T(8,128)(2,1)S(1)}, bf16[128,512]{1,0:T(8,128)(2,1)S(1)}, u32[]{:S(2)}, u32[]{:S(2)}) %collective-permute-start.6) | collective-permute-done | bytes 131104 | tf_op jit(solution)/shard_map/ppermute | solution.py:289
  48.1 0.0 collective-permute-done.5.p1
  48.1 0.9 copy-done.3
  49.0 0.9 copy-done.5
  49.9 0.9 copy-done.7
  50.8 0.9 copy-done.9
  51.7 1.3 %shard_map.118 = (bf16[8,16,640]{2,1,0:T(8,128)(2,1)S(1)}, bf16[2,128,256]{2,1,0:T(8,128)(2,1)S(1)}) custom-call(bf16[128,512]{1,0:T(8,128)(2,1)S(1)} %shard_map.117.p0, bf16[128,512]{1,0:T(8,128)(2,1)S(1)} %collective-permute-done.5.p1, bf16[128,512]{1,0:T(8,128)(2,1)S(1)} %collective-permute-done.6.p2, bf16[128,512]{1,0:T(8,128)(2,1)S(1)} %collective-permute-done.7.p3, ...), custom_call_target="tpu_custom_call" | custom-call | flops 100000000 | bytes 1579008 | tf_op jit(solution)/shard_map/pallas_call | solution.py:25
  53.1 10.7 %all_to_all.20.arrived = bf16[8,16,640]{2,1,0:T(8,128)(2,1)S(1)} all-to-all(bf16[8,16,640]{2,1,0:T(8,128)(2,1)S(1)} %get-tuple-element.19), channel_id=1, replica_groups=mesh['y'=4,'x'=4,'z'=8,'c'=2] {'z'}, dimensions={0} | all-to-all | bytes 327680 | tf_op jit(solution)/shard_map/all_to_all | solution.py:231
  63.7 0.7 shard_map.119
  64.5 12.1 %all_to_all.21 = bf16[32,16,128]{2,1,0:T(8,128)(2,1)S(1)} all-to-all(bf16[32,16,128]{2,1,0:T(8,128)(2,1)S(1)} %get-tuple-element.20), channel_id=1, replica_groups=mesh['y'=4,'x'=4,'z'=8,'c'=2] {'x','z'}, dimensions={0} | all-to-all | bytes 262144 | tf_op jit(solution)/shard_map/all_to_all | solution.py:231
  76.6 0.3 shard_map.120.refs_0_
  76.9 2.0 %collective-permute-start.11 = (bf16[128,512]{1,0:T(8,128)(2,1)S(1)}, bf16[128,512]{1,0:T(8,128)(2,1)S(1)}, u32[]{:S(2)}, u32[]{:S(2)}) collective-permute-start(bf16[128,512]{1,0:T(8,128)(2,1)S(1)} %shard_map.120.refs_0_), channel_id=1, source_target_pairs={{0,192},{64,128},{128,64},{192,0},{1,193},{65,129},{129,65},{193,1... | collective-permute-start | bytes 393224 | tf_op jit(solution)/shard_map/ppermute | solution.py:289
  78.9 0.4 collective-permute-start.10
  79.2 1.0 %collective-permute-start.9 = (bf16[128,512]{1,0:T(8,128)(2,1)S(1)}, bf16[128,512]{1,0:T(8,128)(2,1)S(1)}, u32[]{:S(2)}, u32[]{:S(2)}) collective-permute-start(bf16[128,512]{1,0:T(8,128)(2,1)S(1)} %shard_map.120.refs_0_), channel_id=1, source_target_pairs={{0,64},{64,0},{128,192},{192,128},{1,65},{65,1},{129,193},{193,129... | collective-permute-start | bytes 393224 | tf_op jit(solution)/shard_map/ppermute | solution.py:289
  80.2 2.1 %collective-permute-done.11.refs_3_ = bf16[128,512]{1,0:T(8,128)(2,1)S(1)} collective-permute-done((bf16[128,512]{1,0:T(8,128)(2,1)S(1)}, bf16[128,512]{1,0:T(8,128)(2,1)S(1)}, u32[]{:S(2)}, u32[]{:S(2)}) %collective-permute-start.11) | collective-permute-done | bytes 131104 | tf_op jit(solution)/shard_map/ppermute | solution.py:289
  82.3 1.9 %collective-permute-done.10.refs_2_ = bf16[128,512]{1,0:T(8,128)(2,1)S(1)} collective-permute-done((bf16[128,512]{1,0:T(8,128)(2,1)S(1)}, bf16[128,512]{1,0:T(8,128)(2,1)S(1)}, u32[]{:S(2)}, u32[]{:S(2)}) %collective-permute-start.10) | collective-permute-done | bytes 131104 | tf_op jit(solution)/shard_map/ppermute | solution.py:289
  84.2 0.0 collective-permute-done.9.refs_1_
  84.2 0.1 shard_map.121
  84.3 7.6 %collective-permute-start.12 = (bf16[128,256]{1,0:T(8,128)(2,1)S(1)}, bf16[128,256]{1,0:T(8,128)(2,1)S(1)}, u32[]{:S(2)}, u32[]{:S(2)}) collective-permute-start(bf16[128,256]{1,0:T(8,128)(2,1)S(1)} %get-tuple-element.23), channel_id=1, source_target_pairs={{0,1},{1,0},{2,3},{3,2},{4,5},{5,4},{6,7},{7,6},{8,9},{9,8},{10,11... | collective-permute-start | bytes 196616 | tf_op jit(solution)/shard_map/ppermute | solution.py:243
  91.9 3.2 %new_states.1 = f32[2,16,1,128,128]{4,3,2,1,0:T(8,128)} custom-call(f32[3,16,128]{2,1,0:T(8,128)S(1)} %get-tuple-element.24.terms_a, f32[3,16,128]{2,1,0:T(8,128)S(1)} %get-tuple-element.25.terms_b, f32[2,16,1,128,128]{4,3,2,1,0:T(8,128)S(1)} %copy-done), custom_call_target="tpu_custom_call" | custom-call | flops 10000000 | bytes 4194304 | tf_op jit(solution)/shard_map/new_states/pallas_call | solution.py:203
  95.1 0.0 collective-permute-done.12.received
  95.1 0.7 shard_map.122
  (12 shorter events, 0.0 us)
Async XLA Ops:
  0.6 0.9 copy-start.8
  0.6 1.0 %copy-start.6 = (bf16[2,256,128]{2,1,0:T(8,128)(2,1)S(1)}, bf16[2,256,128]{2,1,0:T(8,128)(2,1)}, u32[]{:S(2)}) copy-start(bf16[2,256,128]{2,1,0:T(8,128)(2,1)} %refs_2_.3) | copy-start | bytes 393220
  0.7 1.0 %copy-start.4 = (bf16[2,256,128]{2,1,0:T(8,128)(2,1)S(1)}, bf16[2,256,128]{2,1,0:T(8,128)(2,1)}, u32[]{:S(2)}) copy-start(bf16[2,256,128]{2,1,0:T(8,128)(2,1)} %refs_1_.3) | copy-start | bytes 393220
  0.7 1.1 %copy-start.2 = (bf16[2,256,128]{2,1,0:T(8,128)(2,1)S(1)}, bf16[2,256,128]{2,1,0:T(8,128)(2,1)}, u32[]{:S(2)}) copy-start(bf16[2,256,128]{2,1,0:T(8,128)(2,1)} %refs_0_.3) | copy-start | bytes 393220
  0.7 1.1 %copy-start.11 = (f32[2,256]{1,0:T(2,128)S(1)}, f32[2,256]{1,0:T(2,128)}, u32[]{:S(2)}) copy-start(f32[2,256]{1,0:T(2,128)} %gain.3) | copy-start | bytes 6148
  0.7 1.1 %copy-start.13 = (f32[2,128]{1,0:T(2,128)S(1)}, f32[2,128]{1,0:T(2,128)}, u32[]{:S(2)}) copy-start(f32[2,128]{1,0:T(2,128)} %head_gain.1) | copy-start | bytes 3076
  0.7 1.0 %copy-start.12 = (f32[2,128]{1,0:T(2,128)S(1)}, f32[2,128]{1,0:T(2,128)}, u32[]{:S(2)}) copy-start(f32[2,128]{1,0:T(2,128)} %floor_rate.1) | copy-start | bytes 3076
  0.7 1.2 %copy-start.1 = (bf16[256,256]{1,0:T(8,128)(2,1)S(1)}, bf16[256,256]{1,0:T(8,128)(2,1)}, u32[]{:S(2)}) copy-start(bf16[256,256]{1,0:T(8,128)(2,1)} %param.10) | copy-start | bytes 393220
  0.7 13.8 %copy-start.15 = (bf16[2,128,256]{2,1,0:T(8,128)(2,1)S(1)}, bf16[2,128,256]{2,1,0:T(8,128)(2,1)}, u32[]{:S(2)}) copy-start(bf16[2,128,256]{2,1,0:T(8,128)(2,1)} %param.18) | copy-start | bytes 393220
  0.7 22.4 %copy-start = (f32[2,16,1,128,128]{4,3,2,1,0:T(8,128)S(1)}, f32[2,16,1,128,128]{4,3,2,1,0:T(8,128)}, u32[]{:S(2)}) copy-start(f32[2,16,1,128,128]{4,3,2,1,0:T(8,128)} %state.5) | copy-start | bytes 6291460
  2.2 0.7 copy-start.14
  2.9 4.2 %collective-permute-start = (bf16[8,16,640]{2,1,0:T(8,128)(2,1)S(1)}, bf16[8,16,640]{2,1,0:T(8,128)(2,1)S(1)}, u32[]{:S(2)}, u32[]{:S(2)}) collective-permute-start(bf16[8,16,640]{2,1,0:T(8,128)(2,1)S(1)} %get-tuple-element.15), channel_id=1, source_target_pairs={{0,1},{1,0},{2,3},{3,2},{4,5},{5,4},{6,7},{7,6},{8,9},{9,8},{10,11... | collective-permute-start | bytes 491528 | tf_op jit(solution)/shard_map/ppermute | solution.py:243
  8.0 15.1 %all-to-all-start = ((bf16[8,16,640]{2,1,0:T(8,128)(2,1)}), bf16[8,16,640]{2,1,0:T(8,128)(2,1)S(1)}, u32[]{:S(2)}, u32[]{:S(2)}) async-start(bf16[8,16,640]{2,1,0:T(8,128)(2,1)} %shard_map.115), calls=%async_computation | async-start | bytes 327680 | tf_op jit(solution)/shard_map/all_to_all | solution.py:231
  14.5 1.7 %collective-permute-start.1 = (bf16[2,128,256]{2,1,0:T(8,128)(2,1)S(1)}, bf16[2,128,256]{2,1,0:T(8,128)(2,1)S(1)}, u32[]{:S(2)}, u32[]{:S(2)}) collective-permute-start(bf16[2,128,256]{2,1,0:T(8,128)(2,1)S(1)} %copy-done.15), channel_id=1, source_target_pairs={{0,1},{1,0},{2,3},{3,2},{4,5},{5,4},{6,7},{7,6},{8,9},{9,8},{10,11... | collective-permute-start | bytes 393224 | tf_op jit(solution)/shard_map/ppermute | solution.py:243
  16.3 15.7 %collective-permute-start.4 = (bf16[2,2,128,256]{3,2,1,0:T(8,128)(2,1)S(1)}, bf16[2,2,128,256]{3,2,1,0:T(8,128)(2,1)S(1)}, u32[]{:S(2)}, u32[]{:S(2)}) collective-permute-start(bf16[2,2,128,256]{3,2,1,0:T(8,128)(2,1)S(1)} %pad_maximum_fusion.refs_0_), channel_id=1, source_target_pairs={{0,48},{16,0},{32,16},{48,32},{1,49},{17,1},{33,17},{49,33},{2,50}... | collective-permute-start | bytes 786440 | tf_op jit(solution)/shard_map/ppermute | solution.py:267
  18.8 13.1 %collective-permute-start.3 = (bf16[2,2,128,256]{3,2,1,0:T(8,128)(2,1)S(1)}, bf16[2,2,128,256]{3,2,1,0:T(8,128)(2,1)S(1)}, u32[]{:S(2)}, u32[]{:S(2)}) collective-permute-start(bf16[2,2,128,256]{3,2,1,0:T(8,128)(2,1)S(1)} %pad_maximum_fusion.refs_0_), channel_id=1, source_target_pairs={{0,32},{16,48},{32,0},{48,16},{1,33},{17,49},{33,1},{49,17},{2,34}... | collective-permute-start | bytes 786440 | tf_op jit(solution)/shard_map/ppermute | solution.py:267
  19.3 14.8 %collective-permute-start.2 = (bf16[2,2,128,256]{3,2,1,0:T(8,128)(2,1)S(1)}, bf16[2,2,128,256]{3,2,1,0:T(8,128)(2,1)S(1)}, u32[]{:S(2)}, u32[]{:S(2)}) collective-permute-start(bf16[2,2,128,256]{3,2,1,0:T(8,128)(2,1)S(1)} %pad_maximum_fusion.refs_0_), channel_id=1, source_target_pairs={{0,16},{16,32},{32,48},{48,0},{1,17},{17,33},{33,49},{49,1},{2,18}... | collective-permute-start | bytes 786440 | tf_op jit(solution)/shard_map/ppermute | solution.py:267
  23.9 0.7 copy-start.10
  24.6 15.0 %all-to-all-start.1 = ((bf16[32,16,128]{2,1,0:T(8,128)(2,1)}), bf16[32,16,128]{2,1,0:T(8,128)(2,1)S(1)}, u32[]{:S(2)}, u32[]{:S(2)}) async-start(bf16[32,16,128]{2,1,0:T(8,128)(2,1)} %copy-done.10), calls=%async_computation.1 | async-start | bytes 262144 | tf_op jit(solution)/shard_map/all_to_all | solution.py:231
  30.4 13.0 %collective-permute-start.8 = (bf16[256,768]{1,0:T(8,128)(2,1)}, bf16[256,768]{1,0:T(8,128)(2,1)}, u32[]{:S(2)}, u32[]{:S(2)}) collective-permute-start(bf16[256,768]{1,0:T(8,128)(2,1)} %copy-done.14), channel_id=1, source_target_pairs={{0,1},{1,0},{2,3},{3,2},{4,5},{5,4},{6,7},{7,6},{8,9},{9,8},{10,11... | collective-permute-start | bytes 1179656 | tf_op jit(solution)/shard_map/ppermute | solution.py:243
  39.8 6.1 %collective-permute-start.7 = (bf16[128,512]{1,0:T(8,128)(2,1)S(1)}, bf16[128,512]{1,0:T(8,128)(2,1)S(1)}, u32[]{:S(2)}, u32[]{:S(2)}) collective-permute-start(bf16[128,512]{1,0:T(8,128)(2,1)S(1)} %shard_map.117.p0), channel_id=1, source_target_pairs={{0,192},{64,128},{128,64},{192,0},{1,193},{65,129},{129,65},{193,1... | collective-permute-start | bytes 393224 | tf_op jit(solution)/shard_map/ppermute | solution.py:289
  42.7 5.4 %collective-permute-start.6 = (bf16[128,512]{1,0:T(8,128)(2,1)S(1)}, bf16[128,512]{1,0:T(8,128)(2,1)S(1)}, u32[]{:S(2)}, u32[]{:S(2)}) collective-permute-start(bf16[128,512]{1,0:T(8,128)(2,1)S(1)} %shard_map.117.p0), channel_id=1, source_target_pairs={{0,128},{64,192},{128,0},{192,64},{1,129},{65,193},{129,1},{193,65... | collective-permute-start | bytes 393224 | tf_op jit(solution)/shard_map/ppermute | solution.py:289
  43.0 5.1 %collective-permute-start.5 = (bf16[128,512]{1,0:T(8,128)(2,1)S(1)}, bf16[128,512]{1,0:T(8,128)(2,1)S(1)}, u32[]{:S(2)}, u32[]{:S(2)}) collective-permute-start(bf16[128,512]{1,0:T(8,128)(2,1)S(1)} %shard_map.117.p0), channel_id=1, source_target_pairs={{0,64},{64,0},{128,192},{192,128},{1,65},{65,1},{129,193},{193,129... | collective-permute-start | bytes 393224 | tf_op jit(solution)/shard_map/ppermute | solution.py:289
  48.1 0.9 copy-start.3
  49.0 0.9 copy-start.5
  49.9 0.9 copy-start.7
  50.8 0.9 copy-start.9
  76.9 5.4 %collective-permute-start.11 = (bf16[128,512]{1,0:T(8,128)(2,1)S(1)}, bf16[128,512]{1,0:T(8,128)(2,1)S(1)}, u32[]{:S(2)}, u32[]{:S(2)}) collective-permute-start(bf16[128,512]{1,0:T(8,128)(2,1)S(1)} %shard_map.120.refs_0_), channel_id=1, source_target_pairs={{0,192},{64,128},{128,64},{192,0},{1,193},{65,129},{129,65},{193,1... | collective-permute-start | bytes 393224 | tf_op jit(solution)/shard_map/ppermute | solution.py:289
  78.9 5.3 %collective-permute-start.10 = (bf16[128,512]{1,0:T(8,128)(2,1)S(1)}, bf16[128,512]{1,0:T(8,128)(2,1)S(1)}, u32[]{:S(2)}, u32[]{:S(2)}) collective-permute-start(bf16[128,512]{1,0:T(8,128)(2,1)S(1)} %shard_map.120.refs_0_), channel_id=1, source_target_pairs={{0,128},{64,192},{128,0},{192,64},{1,129},{65,193},{129,1},{193,65... | collective-permute-start | bytes 393224 | tf_op jit(solution)/shard_map/ppermute | solution.py:289
  79.2 5.0 %collective-permute-start.9 = (bf16[128,512]{1,0:T(8,128)(2,1)S(1)}, bf16[128,512]{1,0:T(8,128)(2,1)S(1)}, u32[]{:S(2)}, u32[]{:S(2)}) collective-permute-start(bf16[128,512]{1,0:T(8,128)(2,1)S(1)} %shard_map.120.refs_0_), channel_id=1, source_target_pairs={{0,64},{64,0},{128,192},{192,128},{1,65},{65,1},{129,193},{193,129... | collective-permute-start | bytes 393224 | tf_op jit(solution)/shard_map/ppermute | solution.py:289
  84.3 10.8 %collective-permute-start.12 = (bf16[128,256]{1,0:T(8,128)(2,1)S(1)}, bf16[128,256]{1,0:T(8,128)(2,1)S(1)}, u32[]{:S(2)}, u32[]{:S(2)}) collective-permute-start(bf16[128,256]{1,0:T(8,128)(2,1)S(1)} %get-tuple-element.23), channel_id=1, source_target_pairs={{0,1},{1,0},{2,3},{3,2},{4,5},{5,4},{6,7},{7,6},{8,9},{9,8},{10,11... | collective-permute-start | bytes 196616 | tf_op jit(solution)/shard_map/ppermute | solution.py:243

commit v2 on v1

--- a/solution.py
+++ b/solution.py
@@ -219,11 +219,15 @@
     rows = heads.shape[1] * heads.shape[2]
     feats = pieces[0].shape[3]
     for half in range(2):
-        total = None
-        for k in range(n_x):
-            head = heads[lax.rem(my_x - k + n_x, n_x)].reshape(rows, LANES)
-            product = jnp.dot(head, pieces[k][half, layer], preferred_element_type=F32)
-            total = product if total is None else total + product
+        products = [
+            jnp.dot(
+                heads[lax.rem(my_x - k + n_x, n_x)].reshape(rows, LANES),
+                pieces[k][half, layer],
+                preferred_element_type=F32,
+            )
+            for k in range(n_x)
+        ]
+        total = (products[0] + products[2]) + (products[1] + products[3])
         out_ref[:, half * feats : (half + 1) * feats] = total.astype(BF16)
 
 

time: 96.2 us -> 96.2 us (level)
  no operation moved by 1% of the time
where the time goes in v2:
time: 96.2 us; the launch traced here: 95.8 us
  starting transfers between devices  35.9 us (37%)
  blocking collectives  22.8 us (24%)
  waiting for transfers between devices  21.6 us (22%)
  Pallas kernels  8.48 us (9%)
  local copies, waits for them, and re-layouts  6.15 us (6%)
    all_to_all x2, blocking collectives, spread(): return lax.all_to_all(copies, axes, split_axis=0, concat_axis=0, tiled=True)  22.8 us
    ppermute x4, starting transfers between devices, swap(): return lax.ppermute(v, 'c', [(0, 1), (1, 0)])  13.1 us
    all_to_all x2, starting transfers between devices, spread(): return lax.all_to_all(copies, axes, split_axis=0, concat_axis=0, tiled=True)  12.3 us
    ppermute x6, waiting for transfers between devices, per_device(): parts.append(lax.ppermute(own, 'y', [(i, i ^ k) for i in range(n_y)]))  8.73 us
    all_to_all x2, waiting for transfers between devices, spread(): return lax.all_to_all(copies, axes, split_axis=0, concat_axis=0, tiled=True)  8.62 us
    ppermute x6, starting transfers between devices, per_device(): parts.append(lax.ppermute(own, 'y', [(i, i ^ k) for i in range(n_y)]))  6.85 us
    unnamed x32, local copies, waits for them, and re-layouts  6.15 us
    pallas_call x10, Pallas kernels, call(): pl.pallas_call(kernel, out_shape=outs, in_specs=[vmem] * len(args), out_s...  5.31 us
  transfers between devices with their start and end apart: 15, of which 9 were waited for; matrix products, arithmetic and copies ran while one was open for 0% of the time, Pallas kernels for 4%

profile of v2, /device:TPU:1, one launch (start us, length us, event | category | flops | bytes accessed | tf_op | source)
XLA Modules:
  0.0 95.8 jit_solution(16080987078896609174)
XLA Ops:
  0.6 0.0 copy-start.8
  0.6 0.0 copy-start.6
  0.7 0.0 copy-start.4
  0.7 0.0 copy-start.2
  0.7 0.0 copy-start.11
  0.7 0.0 copy-start.13
  0.7 0.0 copy-start.12
  0.7 0.0 copy-start.1
  0.7 0.0 copy-start
  0.8 0.8 copy-done.8
  1.5 0.1 copy-done.6
  1.6 0.1 copy-done.4
  1.7 0.1 copy-done.2
  1.7 0.1 copy-done.1
  1.9 0.3 shard_map.114
  2.2 0.0 copy-start.14
  2.2 0.7 copy-done.14
  2.9 3.2 %collective-permute-start = (bf16[8,16,640]{2,1,0:T(8,128)(2,1)S(1)}, bf16[8,16,640]{2,1,0:T(8,128)(2,1)S(1)}, u32[]{:S(2)}, u32[]{:S(2)}) collective-permute-start(bf16[8,16,640]{2,1,0:T(8,128)(2,1)S(1)} %get-tuple-element.15), channel_id=1, source_target_pairs={{0,1},{1,0},{2,3},{3,2},{4,5},{5,4},{6,7},{7,6},{8,9},{9,8},{10,11... | collective-permute-start | bytes 491528 | tf_op jit(solution)/shard_map/ppermute | solution.py:247
  6.1 1.0 %collective-permute-done.received = bf16[8,16,640]{2,1,0:T(8,128)(2,1)S(1)} collective-permute-done((bf16[8,16,640]{2,1,0:T(8,128)(2,1)S(1)}, bf16[8,16,640]{2,1,0:T(8,128)(2,1)S(1)}, u32[]{:S(2)}, u32[]{:S(2)}) %collective-permute-start) | collective-permute-done | bytes 163872 | tf_op jit(solution)/shard_map/ppermute | solution.py:247
  7.2 0.9 shard_map.115
  8.0 6.5 %all-to-all-start = ((bf16[8,16,640]{2,1,0:T(8,128)(2,1)}), bf16[8,16,640]{2,1,0:T(8,128)(2,1)S(1)}, u32[]{:S(2)}, u32[]{:S(2)}) async-start(bf16[8,16,640]{2,1,0:T(8,128)(2,1)} %shard_map.115), calls=%async_computation | async-start | bytes 327680 | tf_op jit(solution)/shard_map/all_to_all | solution.py:235
  14.5 0.7 collective-permute-start.1
  15.3 1.0 %collective-permute-done.1 = bf16[2,128,256]{2,1,0:T(8,128)(2,1)S(1)} collective-permute-done((bf16[2,128,256]{2,1,0:T(8,128)(2,1)S(1)}, bf16[2,128,256]{2,1,0:T(8,128)(2,1)S(1)}, u32[]{:S(2)}, u32[]{:S(2)}) %collective-permute-start.1) | collective-permute-done | bytes 131104 | tf_op jit(solution)/shard_map/ppermute | solution.py:247
  16.3 2.6 %collective-permute-start.4 = (bf16[2,2,128,256]{3,2,1,0:T(8,128)(2,1)S(1)}, bf16[2,2,128,256]{3,2,1,0:T(8,128)(2,1)S(1)}, u32[]{:S(2)}, u32[]{:S(2)}) collective-permute-start(bf16[2,2,128,256]{3,2,1,0:T(8,128)(2,1)S(1)} %pad_maximum_fusion.refs_0_), channel_id=1, source_target_pairs={{0,48},{16,0},{32,16},{48,32},{1,49},{17,1},{33,17},{49,33},{2,50}... | collective-permute-start | bytes 786440 | tf_op jit(solution)/shard_map/ppermute | solution.py:271
  18.8 0.5 collective-permute-start.3
  19.3 0.6 collective-permute-start.2
  19.9 3.2 %all-to-all-done.arrived = bf16[8,16,640]{2,1,0:T(8,128)(2,1)S(1)} async-done(((bf16[8,16,640]{2,1,0:T(8,128)(2,1)}), bf16[8,16,640]{2,1,0:T(8,128)(2,1)S(1)}, u32[]{:S(2)}, u32[]{:S(2)}) %all-to-all-start) | async-done | bytes 163872 | tf_op jit(solution)/shard_map/all_to_all | solution.py:235
  23.2 0.7 shard_map.116
  23.9 0.0 copy-start.10
  23.9 0.6 copy-done.10
  24.6 5.8 %all-to-all-start.1 = ((bf16[32,16,128]{2,1,0:T(8,128)(2,1)}), bf16[32,16,128]{2,1,0:T(8,128)(2,1)S(1)}, u32[]{:S(2)}, u32[]{:S(2)}) async-start(bf16[32,16,128]{2,1,0:T(8,128)(2,1)} %copy-done.10), calls=%async_computation.1 | async-start | bytes 262144 | tf_op jit(solution)/shard_map/all_to_all | solution.py:235
  30.4 1.6 %collective-permute-start.8 = (bf16[256,768]{1,0:T(8,128)(2,1)}, bf16[256,768]{1,0:T(8,128)(2,1)}, u32[]{:S(2)}, u32[]{:S(2)}) collective-permute-start(bf16[256,768]{1,0:T(8,128)(2,1)} %copy-done.14), channel_id=1, source_target_pairs={{0,1},{1,0},{2,3},{3,2},{4,5},{5,4},{6,7},{7,6},{8,9},{9,8},{10,11... | collective-permute-start | bytes 1179656 | tf_op jit(solution)/shard_map/ppermute | solution.py:247
  32.0 0.0 collective-permute-done.4.refs_3_
  32.0 0.0 collective-permute-done.3.refs_2_
  32.0 2.2 %collective-permute-done.2.refs_1_ = bf16[2,2,128,256]{3,2,1,0:T(8,128)(2,1)S(1)} collective-permute-done((bf16[2,2,128,256]{3,2,1,0:T(8,128)(2,1)S(1)}, bf16[2,2,128,256]{3,2,1,0:T(8,128)(2,1)S(1)}, u32[]{:S(2)}, u32[]{:S(2)}) %collective-permute-start.2) | collective-permute-done | bytes 262176 | tf_op jit(solution)/shard_map/ppermute | solution.py:271
  34.2 5.4 %all-to-all-done.1 = bf16[32,16,128]{2,1,0:T(8,128)(2,1)S(1)} async-done(((bf16[32,16,128]{2,1,0:T(8,128)(2,1)}), bf16[32,16,128]{2,1,0:T(8,128)(2,1)S(1)}, u32[]{:S(2)}, u32[]{:S(2)}) %all-to-all-start.1) | async-done | bytes 131104 | tf_op jit(solution)/shard_map/all_to_all | solution.py:235
  39.6 0.3 shard_map.117.p0
  39.8 2.8 %collective-permute-start.7 = (bf16[128,512]{1,0:T(8,128)(2,1)S(1)}, bf16[128,512]{1,0:T(8,128)(2,1)S(1)}, u32[]{:S(2)}, u32[]{:S(2)}) collective-permute-start(bf16[128,512]{1,0:T(8,128)(2,1)S(1)} %shard_map.117.p0), channel_id=1, source_target_pairs={{0,192},{64,128},{128,64},{192,0},{1,193},{65,129},{129,65},{193,1... | collective-permute-start | bytes 393224 | tf_op jit(solution)/shard_map/ppermute | solution.py:293
  42.7 0.4 collective-permute-start.6
  43.0 0.3 collective-permute-start.5
  43.4 0.0 collective-permute-done.8.refs_4_
  43.4 2.6 %collective-permute-done.7.p3 = bf16[128,512]{1,0:T(8,128)(2,1)S(1)} collective-permute-done((bf16[128,512]{1,0:T(8,128)(2,1)S(1)}, bf16[128,512]{1,0:T(8,128)(2,1)S(1)}, u32[]{:S(2)}, u32[]{:S(2)}) %collective-permute-start.7) | collective-permute-done | bytes 131104 | tf_op jit(solution)/shard_map/ppermute | solution.py:293
  46.0 2.1 %collective-permute-done.6.p2 = bf16[128,512]{1,0:T(8,128)(2,1)S(1)} collective-permute-done((bf16[128,512]{1,0:T(8,128)(2,1)S(1)}, bf16[128,512]{1,0:T(8,128)(2,1)S(1)}, u32[]{:S(2)}, u32[]{:S(2)}) %collective-permute-start.6) | collective-permute-done | bytes 131104 | tf_op jit(solution)/shard_map/ppermute | solution.py:293
  48.1 0.0 collective-permute-done.5.p1
  48.1 0.9 copy-done.3
  49.0 0.9 copy-done.5
  49.9 0.9 copy-done.7
  50.8 0.9 copy-done.9
  51.7 1.3 %shard_map.118 = (bf16[8,16,640]{2,1,0:T(8,128)(2,1)S(1)}, bf16[2,128,256]{2,1,0:T(8,128)(2,1)S(1)}) custom-call(bf16[128,512]{1,0:T(8,128)(2,1)S(1)} %shard_map.117.p0, bf16[128,512]{1,0:T(8,128)(2,1)S(1)} %collective-permute-done.5.p1, bf16[128,512]{1,0:T(8,128)(2,1)S(1)} %collective-permute-done.6.p2, bf16[128,512]{1,0:T(8,128)(2,1)S(1)} %collective-permute-done.7.p3, ...), custom_call_target="tpu_custom_call" | custom-call | flops 100000000 | bytes 1579008 | tf_op jit(solution)/shard_map/pallas_call | solution.py:25
  53.1 10.7 %all_to_all.20.arrived = bf16[8,16,640]{2,1,0:T(8,128)(2,1)S(1)} all-to-all(bf16[8,16,640]{2,1,0:T(8,128)(2,1)S(1)} %get-tuple-element.19), channel_id=1, replica_groups=mesh['y'=4,'x'=4,'z'=8,'c'=2] {'z'}, dimensions={0} | all-to-all | bytes 327680 | tf_op jit(solution)/shard_map/all_to_all | solution.py:235
  63.7 0.7 shard_map.119
  64.5 12.1 %all_to_all.21 = bf16[32,16,128]{2,1,0:T(8,128)(2,1)S(1)} all-to-all(bf16[32,16,128]{2,1,0:T(8,128)(2,1)S(1)} %get-tuple-element.20), channel_id=1, replica_groups=mesh['y'=4,'x'=4,'z'=8,'c'=2] {'x','z'}, dimensions={0} | all-to-all | bytes 262144 | tf_op jit(solution)/shard_map/all_to_all | solution.py:235
  76.6 0.3 shard_map.120.refs_0_
  76.9 2.0 %collective-permute-start.11 = (bf16[128,512]{1,0:T(8,128)(2,1)S(1)}, bf16[128,512]{1,0:T(8,128)(2,1)S(1)}, u32[]{:S(2)}, u32[]{:S(2)}) collective-permute-start(bf16[128,512]{1,0:T(8,128)(2,1)S(1)} %shard_map.120.refs_0_), channel_id=1, source_target_pairs={{0,192},{64,128},{128,64},{192,0},{1,193},{65,129},{129,65},{193,1... | collective-permute-start | bytes 393224 | tf_op jit(solution)/shard_map/ppermute | solution.py:293
  78.9 0.4 collective-permute-start.10
  79.2 1.0 %collective-permute-start.9 = (bf16[128,512]{1,0:T(8,128)(2,1)S(1)}, bf16[128,512]{1,0:T(8,128)(2,1)S(1)}, u32[]{:S(2)}, u32[]{:S(2)}) collective-permute-start(bf16[128,512]{1,0:T(8,128)(2,1)S(1)} %shard_map.120.refs_0_), channel_id=1, source_target_pairs={{0,64},{64,0},{128,192},{192,128},{1,65},{65,1},{129,193},{193,129... | collective-permute-start | bytes 393224 | tf_op jit(solution)/shard_map/ppermute | solution.py:293
  80.2 2.1 %collective-permute-done.11.refs_3_ = bf16[128,512]{1,0:T(8,128)(2,1)S(1)} collective-permute-done((bf16[128,512]{1,0:T(8,128)(2,1)S(1)}, bf16[128,512]{1,0:T(8,128)(2,1)S(1)}, u32[]{:S(2)}, u32[]{:S(2)}) %collective-permute-start.11) | collective-permute-done | bytes 131104 | tf_op jit(solution)/shard_map/ppermute | solution.py:293
  82.3 1.9 %collective-permute-done.10.refs_2_ = bf16[128,512]{1,0:T(8,128)(2,1)S(1)} collective-permute-done((bf16[128,512]{1,0:T(8,128)(2,1)S(1)}, bf16[128,512]{1,0:T(8,128)(2,1)S(1)}, u32[]{:S(2)}, u32[]{:S(2)}) %collective-permute-start.10) | collective-permute-done | bytes 131104 | tf_op jit(solution)/shard_map/ppermute | solution.py:293
  84.2 0.0 collective-permute-done.9.refs_1_
  84.2 0.1 shard_map.121
  84.3 7.6 %collective-permute-start.12 = (bf16[128,256]{1,0:T(8,128)(2,1)S(1)}, bf16[128,256]{1,0:T(8,128)(2,1)S(1)}, u32[]{:S(2)}, u32[]{:S(2)}) collective-permute-start(bf16[128,256]{1,0:T(8,128)(2,1)S(1)} %get-tuple-element.23), channel_id=1, source_target_pairs={{0,1},{1,0},{2,3},{3,2},{4,5},{5,4},{6,7},{7,6},{8,9},{9,8},{10,11... | collective-permute-start | bytes 196616 | tf_op jit(solution)/shard_map/ppermute | solution.py:247
  91.9 3.2 %new_states.1 = f32[2,16,1,128,128]{4,3,2,1,0:T(8,128)} custom-call(f32[3,16,128]{2,1,0:T(8,128)S(1)} %get-tuple-element.24.terms_a, f32[3,16,128]{2,1,0:T(8,128)S(1)} %get-tuple-element.25.terms_b, f32[2,16,1,128,128]{4,3,2,1,0:T(8,128)S(1)} %copy-done), custom_call_target="tpu_custom_call" | custom-call | flops 10000000 | bytes 4194304 | tf_op jit(solution)/shard_map/new_states/pallas_call | solution.py:203
  95.1 0.0 collective-permute-done.12.received
  95.1 0.7 shard_map.122
  (12 shorter events, 0.0 us)
Async XLA Ops:
  0.6 0.9 copy-start.8
  0.6 1.0 %copy-start.6 = (bf16[2,256,128]{2,1,0:T(8,128)(2,1)S(1)}, bf16[2,256,128]{2,1,0:T(8,128)(2,1)}, u32[]{:S(2)}) copy-start(bf16[2,256,128]{2,1,0:T(8,128)(2,1)} %refs_2_.3) | copy-start | bytes 393220
  0.7 1.0 %copy-start.4 = (bf16[2,256,128]{2,1,0:T(8,128)(2,1)S(1)}, bf16[2,256,128]{2,1,0:T(8,128)(2,1)}, u32[]{:S(2)}) copy-start(bf16[2,256,128]{2,1,0:T(8,128)(2,1)} %refs_1_.3) | copy-start | bytes 393220
  0.7 1.1 %copy-start.2 = (bf16[2,256,128]{2,1,0:T(8,128)(2,1)S(1)}, bf16[2,256,128]{2,1,0:T(8,128)(2,1)}, u32[]{:S(2)}) copy-start(bf16[2,256,128]{2,1,0:T(8,128)(2,1)} %refs_0_.3) | copy-start | bytes 393220
  0.7 1.1 %copy-start.11 = (f32[2,256]{1,0:T(2,128)S(1)}, f32[2,256]{1,0:T(2,128)}, u32[]{:S(2)}) copy-start(f32[2,256]{1,0:T(2,128)} %gain.3) | copy-start | bytes 6148
  0.7 1.1 %copy-start.13 = (f32[2,128]{1,0:T(2,128)S(1)}, f32[2,128]{1,0:T(2,128)}, u32[]{:S(2)}) copy-start(f32[2,128]{1,0:T(2,128)} %head_gain.1) | copy-start | bytes 3076
  0.7 1.0 %copy-start.12 = (f32[2,128]{1,0:T(2,128)S(1)}, f32[2,128]{1,0:T(2,128)}, u32[]{:S(2)}) copy-start(f32[2,128]{1,0:T(2,128)} %floor_rate.1) | copy-start | bytes 3076
  0.7 1.2 %copy-start.1 = (bf16[256,256]{1,0:T(8,128)(2,1)S(1)}, bf16[256,256]{1,0:T(8,128)(2,1)}, u32[]{:S(2)}) copy-start(bf16[256,256]{1,0:T(8,128)(2,1)} %param.10) | copy-start | bytes 393220
  0.7 13.8 %copy-start.15 = (bf16[2,128,256]{2,1,0:T(8,128)(2,1)S(1)}, bf16[2,128,256]{2,1,0:T(8,128)(2,1)}, u32[]{:S(2)}) copy-start(bf16[2,128,256]{2,1,0:T(8,128)(2,1)} %param.18) | copy-start | bytes 393220
  0.7 22.4 %copy-start = (f32[2,16,1,128,128]{4,3,2,1,0:T(8,128)S(1)}, f32[2,16,1,128,128]{4,3,2,1,0:T(8,128)}, u32[]{:S(2)}) copy-start(f32[2,16,1,128,128]{4,3,2,1,0:T(8,128)} %state.5) | copy-start | bytes 6291460
  2.2 0.7 copy-start.14
  2.9 4.2 %collective-permute-start = (bf16[8,16,640]{2,1,0:T(8,128)(2,1)S(1)}, bf16[8,16,640]{2,1,0:T(8,128)(2,1)S(1)}, u32[]{:S(2)}, u32[]{:S(2)}) collective-permute-start(bf16[8,16,640]{2,1,0:T(8,128)(2,1)S(1)} %get-tuple-element.15), channel_id=1, source_target_pairs={{0,1},{1,0},{2,3},{3,2},{4,5},{5,4},{6,7},{7,6},{8,9},{9,8},{10,11... | collective-permute-start | bytes 491528 | tf_op jit(solution)/shard_map/ppermute | solution.py:247
  8.0 15.1 %all-to-all-start = ((bf16[8,16,640]{2,1,0:T(8,128)(2,1)}), bf16[8,16,640]{2,1,0:T(8,128)(2,1)S(1)}, u32[]{:S(2)}, u32[]{:S(2)}) async-start(bf16[8,16,640]{2,1,0:T(8,128)(2,1)} %shard_map.115), calls=%async_computation | async-start | bytes 327680 | tf_op jit(solution)/shard_map/all_to_all | solution.py:235
  14.5 1.7 %collective-permute-start.1 = (bf16[2,128,256]{2,1,0:T(8,128)(2,1)S(1)}, bf16[2,128,256]{2,1,0:T(8,128)(2,1)S(1)}, u32[]{:S(2)}, u32[]{:S(2)}) collective-permute-start(bf16[2,128,256]{2,1,0:T(8,128)(2,1)S(1)} %copy-done.15), channel_id=1, source_target_pairs={{0,1},{1,0},{2,3},{3,2},{4,5},{5,4},{6,7},{7,6},{8,9},{9,8},{10,11... | collective-permute-start | bytes 393224 | tf_op jit(solution)/shard_map/ppermute | solution.py:247
  16.3 15.7 %collective-permute-start.4 = (bf16[2,2,128,256]{3,2,1,0:T(8,128)(2,1)S(1)}, bf16[2,2,128,256]{3,2,1,0:T(8,128)(2,1)S(1)}, u32[]{:S(2)}, u32[]{:S(2)}) collective-permute-start(bf16[2,2,128,256]{3,2,1,0:T(8,128)(2,1)S(1)} %pad_maximum_fusion.refs_0_), channel_id=1, source_target_pairs={{0,48},{16,0},{32,16},{48,32},{1,49},{17,1},{33,17},{49,33},{2,50}... | collective-permute-start | bytes 786440 | tf_op jit(solution)/shard_map/ppermute | solution.py:271
  18.8 13.1 %collective-permute-start.3 = (bf16[2,2,128,256]{3,2,1,0:T(8,128)(2,1)S(1)}, bf16[2,2,128,256]{3,2,1,0:T(8,128)(2,1)S(1)}, u32[]{:S(2)}, u32[]{:S(2)}) collective-permute-start(bf16[2,2,128,256]{3,2,1,0:T(8,128)(2,1)S(1)} %pad_maximum_fusion.refs_0_), channel_id=1, source_target_pairs={{0,32},{16,48},{32,0},{48,16},{1,33},{17,49},{33,1},{49,17},{2,34}... | collective-permute-start | bytes 786440 | tf_op jit(solution)/shard_map/ppermute | solution.py:271
  19.3 14.8 %collective-permute-start.2 = (bf16[2,2,128,256]{3,2,1,0:T(8,128)(2,1)S(1)}, bf16[2,2,128,256]{3,2,1,0:T(8,128)(2,1)S(1)}, u32[]{:S(2)}, u32[]{:S(2)}) collective-permute-start(bf16[2,2,128,256]{3,2,1,0:T(8,128)(2,1)S(1)} %pad_maximum_fusion.refs_0_), channel_id=1, source_target_pairs={{0,16},{16,32},{32,48},{48,0},{1,17},{17,33},{33,49},{49,1},{2,18}... | collective-permute-start | bytes 786440 | tf_op jit(solution)/shard_map/ppermute | solution.py:271
  23.9 0.7 copy-start.10
  24.6 15.0 %all-to-all-start.1 = ((bf16[32,16,128]{2,1,0:T(8,128)(2,1)}), bf16[32,16,128]{2,1,0:T(8,128)(2,1)S(1)}, u32[]{:S(2)}, u32[]{:S(2)}) async-start(bf16[32,16,128]{2,1,0:T(8,128)(2,1)} %copy-done.10), calls=%async_computation.1 | async-start | bytes 262144 | tf_op jit(solution)/shard_map/all_to_all | solution.py:235
  30.4 13.0 %collective-permute-start.8 = (bf16[256,768]{1,0:T(8,128)(2,1)}, bf16[256,768]{1,0:T(8,128)(2,1)}, u32[]{:S(2)}, u32[]{:S(2)}) collective-permute-start(bf16[256,768]{1,0:T(8,128)(2,1)} %copy-done.14), channel_id=1, source_target_pairs={{0,1},{1,0},{2,3},{3,2},{4,5},{5,4},{6,7},{7,6},{8,9},{9,8},{10,11... | collective-permute-start | bytes 1179656 | tf_op jit(solution)/shard_map/ppermute | solution.py:247
  39.8 6.1 %collective-permute-start.7 = (bf16[128,512]{1,0:T(8,128)(2,1)S(1)}, bf16[128,512]{1,0:T(8,128)(2,1)S(1)}, u32[]{:S(2)}, u32[]{:S(2)}) collective-permute-start(bf16[128,512]{1,0:T(8,128)(2,1)S(1)} %shard_map.117.p0), channel_id=1, source_target_pairs={{0,192},{64,128},{128,64},{192,0},{1,193},{65,129},{129,65},{193,1... | collective-permute-start | bytes 393224 | tf_op jit(solution)/shard_map/ppermute | solution.py:293
  42.7 5.4 %collective-permute-start.6 = (bf16[128,512]{1,0:T(8,128)(2,1)S(1)}, bf16[128,512]{1,0:T(8,128)(2,1)S(1)}, u32[]{:S(2)}, u32[]{:S(2)}) collective-permute-start(bf16[128,512]{1,0:T(8,128)(2,1)S(1)} %shard_map.117.p0), channel_id=1, source_target_pairs={{0,128},{64,192},{128,0},{192,64},{1,129},{65,193},{129,1},{193,65... | collective-permute-start | bytes 393224 | tf_op jit(solution)/shard_map/ppermute | solution.py:293
  43.0 5.1 %collective-permute-start.5 = (bf16[128,512]{1,0:T(8,128)(2,1)S(1)}, bf16[128,512]{1,0:T(8,128)(2,1)S(1)}, u32[]{:S(2)}, u32[]{:S(2)}) collective-permute-start(bf16[128,512]{1,0:T(8,128)(2,1)S(1)} %shard_map.117.p0), channel_id=1, source_target_pairs={{0,64},{64,0},{128,192},{192,128},{1,65},{65,1},{129,193},{193,129... | collective-permute-start | bytes 393224 | tf_op jit(solution)/shard_map/ppermute | solution.py:293
  48.1 0.9 copy-start.3
  49.0 0.9 copy-start.5
  49.9 0.9 copy-start.7
  50.8 0.9 copy-start.9
  76.9 5.4 %collective-permute-start.11 = (bf16[128,512]{1,0:T(8,128)(2,1)S(1)}, bf16[128,512]{1,0:T(8,128)(2,1)S(1)}, u32[]{:S(2)}, u32[]{:S(2)}) collective-permute-start(bf16[128,512]{1,0:T(8,128)(2,1)S(1)} %shard_map.120.refs_0_), channel_id=1, source_target_pairs={{0,192},{64,128},{128,64},{192,0},{1,193},{65,129},{129,65},{193,1... | collective-permute-start | bytes 393224 | tf_op jit(solution)/shard_map/ppermute | solution.py:293
  78.9 5.3 %collective-permute-start.10 = (bf16[128,512]{1,0:T(8,128)(2,1)S(1)}, bf16[128,512]{1,0:T(8,128)(2,1)S(1)}, u32[]{:S(2)}, u32[]{:S(2)}) collective-permute-start(bf16[128,512]{1,0:T(8,128)(2,1)S(1)} %shard_map.120.refs_0_), channel_id=1, source_target_pairs={{0,128},{64,192},{128,0},{192,64},{1,129},{65,193},{129,1},{193,65... | collective-permute-start | bytes 393224 | tf_op jit(solution)/shard_map/ppermute | solution.py:293
  79.2 5.0 %collective-permute-start.9 = (bf16[128,512]{1,0:T(8,128)(2,1)S(1)}, bf16[128,512]{1,0:T(8,128)(2,1)S(1)}, u32[]{:S(2)}, u32[]{:S(2)}) collective-permute-start(bf16[128,512]{1,0:T(8,128)(2,1)S(1)} %shard_map.120.refs_0_), channel_id=1, source_target_pairs={{0,64},{64,0},{128,192},{192,128},{1,65},{65,1},{129,193},{193,129... | collective-permute-start | bytes 393224 | tf_op jit(solution)/shard_map/ppermute | solution.py:293
  84.3 10.8 %collective-permute-start.12 = (bf16[128,256]{1,0:T(8,128)(2,1)S(1)}, bf16[128,256]{1,0:T(8,128)(2,1)S(1)}, u32[]{:S(2)}, u32[]{:S(2)}) collective-permute-start(bf16[128,256]{1,0:T(8,128)(2,1)S(1)} %get-tuple-element.23), channel_id=1, source_target_pairs={{0,1},{1,0},{2,3},{3,2},{4,5},{5,4},{6,7},{7,6},{8,9},{9,8},{10,11... | collective-permute-start | bytes 196616 | tf_op jit(solution)/shard_map/ppermute | solution.py:247
